TPU v7x, 32 devices: a whole 2x2x4 slice. The times are simulated.
32 devices in a mesh: fs: 8 (over z, core), tp: 4 (over y, x).
Axes of the slice: x: 2, y: 2, z: 4, core: 2. Of those that a mesh axis runs over, the one named last changes fastest.
Arguments:
- rows_later: bfloat16 [6144, 2048], P('fs'), may hold values from -6 to 6
- rows_earlier: bfloat16 [6144, 2048], P('fs'), may hold values from -6 to 6
- out_cotangent: bfloat16 [6144, 4096], P('fs', 'tp'), may hold values from -6 to 6
- gate_proj: bfloat16 [2048, 4096], P('fs', 'tp'), may hold values from -0.125 to 0.125
- up_proj: bfloat16 [2048, 4096], P('fs', 'tp'), may hold values from -0.125 to 0.125
- conv_taps: float32 [3, 4096], P(None, 'tp'), may hold values from -4 to 4
- conv_bias: float32 [4096], P('tp'), may hold values from -3 to 3
- gate_grad_sum: float32 [2048, 4096], P('fs', 'tp'), may hold values from -6 to 6
- up_grad_sum: float32 [2048, 4096], P('fs', 'tp'), may hold values from -6 to 6
- taps_grad_sum: float32 [3, 4096], P(None, 'tp'), may hold values from -6 to 6
- bias_grad_sum: float32 [4096], P('tp'), may hold values from -6 to 6
Outputs:
- hidden_later: bfloat16 [6144, 4096], P('fs', 'tp')
- input_grad: bfloat16 [6144, 2048], P('fs')
- gate_grad_out: float32 [2048, 4096], P('fs', 'tp')
- up_grad_out: float32 [2048, 4096], P('fs', 'tp')
- taps_grad_out: float32 [3, 4096], P(None, 'tp')
- bias_grad_out: float32 [4096], P('tp')
All inputs are finite; a program needn't handle non-finite values.
Results may differ from a plain program's by a relative error of at most 0.019.
Values may be sent and summed in bfloat16 or wider, within the bound.
A program may use at most 128 MiB of HBM per device.

v0:
```python
import functools
import math

import jax
import jax.numpy as jnp
from jax import lax
from jax.experimental import pallas as pl
from jax.experimental.pallas import tpu as pltpu
from jax.sharding import PartitionSpec as P

MESH = pl.DeviceIdType.MESH
VMEM_BYTES = 58 * 1024 * 1024


def add_parts(target, parts, block):
    width = target.shape[-1]
    block = min(block, width)

    def body(index, carry):
        columns = pl.ds(pl.multiple_of(index * block, block), block)
        total = parts[0][:, columns].astype(jnp.float32)
        for part in parts[1:]:
            total += part[:, columns].astype(jnp.float32)
        target[:, columns] = total.astype(target.dtype)
        return carry

    lax.fori_loop(0, width // block, body, 0)


def reduce_kernel(
    chips,
    side,
    earlier_ref,
    gate_grad_ref,
    up_grad_ref,
    weights_ref,
    small_ref,
    gate_out,
    up_out,
    rows_out,
    small_out,
    terms,
    rows_ref,
    ring,
    pair,
    first_in,
    first_sum,
    second_in,
    rows_buf,
    small_buf,
    ring_send,
    ring_recv,
    pair_send,
    pair_recv,
    first_send,
    first_recv,
    second_send,
    second_recv,
    third_send,
    third_recv,
    fourth_send,
    fourth_recv,
    small_send,
    small_recv,
):
    fs = lax.axis_index("fs")
    tp = lax.axis_index("tp")
    fs_size = 2 * chips
    z = fs // 2
    core = lax.rem(fs, 2)
    partner = z * 2 + 1 - core
    ty = tp // side
    tx = lax.rem(tp, side)
    firsts = (tx, ty)
    seconds = (ty, tx)

    def first_peer(half, k):
        peer = lax.rem(firsts[half] + k, side)
        return peer, (ty * side + peer if half == 0 else peer * side + tx)

    def second_peer(half, k):
        peer = lax.rem(seconds[half] + k, side)
        return peer, (peer * side + tx if half == 0 else ty * side + peer)

    barrier = pltpu.get_barrier_semaphore()
    for k in range(1, fs_size):
        pl.semaphore_signal(
            barrier, inc=1, device_id={"fs": lax.rem(fs + k, fs_size)}, device_id_type=MESH
        )
    for half in range(2):
        for k in range(1, side):
            pl.semaphore_signal(
                barrier, inc=1, device_id={"tp": first_peer(half, k)[1]}, device_id_type=MESH
            )
    pl.semaphore_wait(barrier, fs_size - 1 + 2 * (side - 1))

    parts = (terms.at[0], terms.at[1])
    grad_refs = (gate_grad_ref, up_grad_ref)
    outs = (gate_out, up_out)
    depth = terms.shape[2]
    wide = depth if depth % 128 == 0 else 2 * depth

    def make_terms(d, half):
        for piece in range(2 * depth // wide):
            start = pl.multiple_of(d * 2 * depth + piece * wide, wide)
            value = contract_first(earlier_ref[:, pl.ds(start, wide)], grad_refs[half][...])
            for index in range(wide // depth):
                rows = value[index * depth : (index + 1) * depth]
                terms[half, 2 * d + piece + index] = rows.astype(terms.dtype)

    def make_rows():
        model = weights_ref.shape[1]
        step = min(256, model)
        r = rows_ref.shape[3]

        def body(index, carry):
            columns = pl.ds(pl.multiple_of(index * step, step), step)
            value = contract_last(gate_grad_ref[...], weights_ref[0, columns])
            value += contract_last(up_grad_ref[...], weights_ref[1, columns])
            value = value.astype(rows_ref.dtype)
            for half in range(2):
                for i in range(side):
                    for j in range(side):
                        at = ((half * side + i) * side + j) * r
                        rows_ref[half, i, j, :, columns] = value[at : at + r]
            return carry

        lax.fori_loop(0, model // step, body, 0)

    def pair_copy(d, half):
        return pltpu.make_async_remote_copy(
            src_ref=parts[half].at[2 * d + 1 - core],
            dst_ref=pair.at[d, half],
            send_sem=pair_send.at[d, half],
            recv_sem=pair_recv.at[d, half],
            device_id={"fs": partner},
            device_id_type=MESH,
        )

    def ring_copy(way, d, half):
        target = lax.rem(fs + (2 if way == 0 else fs_size - 2), fs_size)
        return pltpu.make_async_remote_copy(
            src_ref=ring.at[way, d, half],
            dst_ref=ring.at[way, d, half],
            send_sem=ring_send.at[way, d, half],
            recv_sem=ring_recv.at[way, d, half],
            device_id={"fs": target},
            device_id_type=MESH,
        )

    def first_copy(half, k):
        peer, device = first_peer(half, k)
        return pltpu.make_async_remote_copy(
            src_ref=rows_ref.at[half, peer],
            dst_ref=first_in.at[half, k - 1],
            send_sem=first_send.at[half, k - 1],
            recv_sem=first_recv.at[half, k - 1],
            device_id={"tp": device},
            device_id_type=MESH,
        )

    def second_copy(half, k):
        peer, device = second_peer(half, k)
        return pltpu.make_async_remote_copy(
            src_ref=first_sum.at[half, peer],
            dst_ref=second_in.at[half, k - 1],
            send_sem=second_send.at[half, k - 1],
            recv_sem=second_recv.at[half, k - 1],
            device_id={"tp": device},
            device_id_type=MESH,
        )

    def third_copy(half, k, shown):
        _, device = second_peer(half, k)
        block = rows_buf.at[half, firsts[half], shown]
        return pltpu.make_async_remote_copy(
            src_ref=block,
            dst_ref=block,
            send_sem=third_send.at[half, k - 1],
            recv_sem=third_recv.at[half, k - 1],
            device_id={"tp": device},
            device_id_type=MESH,
        )

    def fourth_copy(half, k, shown):
        _, device = first_peer(half, k)
        block = rows_buf.at[half, shown]
        return pltpu.make_async_remote_copy(
            src_ref=block,
            dst_ref=block,
            send_sem=fourth_send.at[half, k - 1],
            recv_sem=fourth_recv.at[half, k - 1],
            device_id={"tp": device},
            device_id_type=MESH,
        )

    def small_copy(k, slot):
        return pltpu.make_async_remote_copy(
            src_ref=small_ref,
            dst_ref=small_buf.at[slot],
            send_sem=small_send.at[k - 1],
            recv_sem=small_recv.at[k - 1],
            device_id={"fs": lax.rem(fs + k, fs_size)},
            device_id_type=MESH,
        )

    def start_first():
        for k in range(1, side):
            for half in range(2):
                first_copy(half, k).start()

    def start_second():
        for half in range(2):
            for k in range(1, side):
                first_copy(half, k).wait_recv()
            for j in range(side):
                add_parts(
                    first_sum.at[half, j],
                    [rows_ref.at[half, firsts[half], j]]
                    + [first_in.at[half, k, j] for k in range(side - 1)],
                    256,
                )
            for k in range(1, side):
                second_copy(half, k).start()

    def start_third():
        for half in range(2):
            for k in range(1, side):
                second_copy(half, k).wait_recv()
            add_parts(
                rows_buf.at[half, firsts[half], seconds[half]],
                [first_sum.at[half, seconds[half]]]
                + [second_in.at[half, k] for k in range(side - 1)],
                256,
            )
            for k in range(1, side):
                third_copy(half, k, seconds[half]).start()

    def start_fourth():
        for half in range(2):
            for k in range(1, side):
                third_copy(half, k, lax.rem(seconds[half] + side - k, side)).wait_recv()
            for k in range(1, side):
                fourth_copy(half, k, firsts[half]).start()

    def finish_rows():
        for half in range(2):
            for k in range(1, side):
                fourth_copy(half, k, lax.rem(firsts[half] + side - k, side)).wait_recv()
        for half in range(2):
            for i in range(side):
                for j in range(side):
                    add_parts(rows_out.at[half, i, j], [rows_buf.at[half, i, j]], 256)

    def own(d, half):
        return parts[half].at[2 * d + core]

    def push(way, d, half, first_on_line):
        pair_copy(d, half).wait_recv()
        slot = ring.at[way, d, half]

        @pl.when(first_on_line)
        def _():
            add_parts(slot, [own(d, half), pair.at[d, half]], 128)

        @pl.when(jnp.logical_not(first_on_line))
        def _():
            ring_copy(way, d, half).wait_recv()
            add_parts(slot, [own(d, half), pair.at[d, half], slot], 128)

        ring_copy(way, d, half).start()

    last = chips - 1

    def ring_step(t, half):
        if t < last:

            @pl.when(t >= z)
            def _():
                push(0, last - t + z, half, z == 0)

            @pl.when(t >= last - z)
            def _():
                push(1, t - last + z, half, z == last)

            return
        pair_copy(z, half).wait_recv()
        target = outs[half]
        base = [own(z, half), pair.at[z, half]]

        @pl.when(z > 0)
        def _():
            ring_copy(0, z, half).wait_recv()

        @pl.when(z < last)
        def _():
            ring_copy(1, z, half).wait_recv()

        @pl.when(z == 0)
        def _():
            add_parts(target, base + [ring.at[1, z, half]], 128)

        @pl.when(z == last)
        def _():
            add_parts(target, base + [ring.at[0, z, half]], 128)

        @pl.when(jnp.logical_and(z > 0, z < last))
        def _():
            add_parts(target, base + [ring.at[0, z, half], ring.at[1, z, half]], 128)

    def in_turn(k):
        return jnp.where(z < chips // 2, last - k, k)

    for half in range(2):
        make_terms(in_turn(0), half)
        pair_copy(in_turn(0), half).start()
    small_buf[fs] = small_ref[...]
    for half in range(2):
        ring_step(0, half)
    make_rows()
    start_first()
    for k in range(1, chips):
        for half in range(2):
            make_terms(in_turn(k), half)
            pair_copy(in_turn(k), half).start()
    for k in range(1, fs_size):
        small_copy(k, fs).start()
    stages = {3: start_second, 4: start_third, 5: start_fourth, 6: finish_rows}
    for t in range(1, chips):
        for half in range(2):
            ring_step(t, half)
            if 2 * t + half in stages:
                stages[2 * t + half]()

    for k in range(1, fs_size):
        small_copy(k, lax.rem(fs + fs_size - k, fs_size)).wait_recv()
    total = small_buf[0]
    for source in range(1, fs_size):
        total += small_buf[source]
    small_out[...] = total

    for half in range(2):
        for d in range(chips):
            pair_copy(d, half).wait_send()
        for k in range(1, side):
            first_copy(half, k).wait_send()
            second_copy(half, k).wait_send()
            third_copy(half, k, seconds[half]).wait_send()
            fourth_copy(half, k, firsts[half]).wait_send()
        for d in range(chips):

            @pl.when(z < d)
            def _():
                ring_copy(0, d, half).wait_send()

            @pl.when(z > d)
            def _():
                ring_copy(1, d, half).wait_send()

    for k in range(1, fs_size):
        small_copy(k, fs).wait_send()


def reduce_all(rows_earlier, gate_grad, up_grad, weights, small):
    fs_size = lax.axis_size("fs")
    chips = fs_size // 2
    side = math.isqrt(lax.axis_size("tp"))
    tokens, model = rows_earlier.shape
    depth, width = model // fs_size, gate_grad.shape[1]
    r = tokens // (2 * side * side)
    bf16, dma = jnp.bfloat16, pltpu.SemaphoreType.DMA
    vmem = pl.BlockSpec(memory_space=pltpu.VMEM)
    rows_shape = (2, side, side, r, model)
    gate_sum, up_sum, rows, small_sum = pl.pallas_call(
        functools.partial(reduce_kernel, chips, side),
        out_shape=(
            jax.ShapeDtypeStruct((depth, width), jnp.float32),
            jax.ShapeDtypeStruct((depth, width), jnp.float32),
            jax.ShapeDtypeStruct(rows_shape, bf16),
            jax.ShapeDtypeStruct(small.shape, jnp.float32),
        ),
        in_specs=[vmem] * 5,
        out_specs=(vmem, vmem, vmem, vmem),
        scratch_shapes=[
            pltpu.VMEM((2, fs_size, depth, width), bf16),
            pltpu.VMEM(rows_shape, bf16),
            pltpu.VMEM((2, chips, 2, depth, width), bf16),
            pltpu.VMEM((chips, 2, depth, width), bf16),
            pltpu.VMEM((2, side - 1, side, r, model), bf16),
            pltpu.VMEM((2, side, r, model), bf16),
            pltpu.VMEM((2, side - 1, r, model), bf16),
            pltpu.VMEM(rows_shape, bf16),
            pltpu.VMEM((fs_size,) + small.shape, jnp.float32),
            dma((2, chips, 2)),
            dma((2, chips, 2)),
            dma((chips, 2)),
            dma((chips, 2)),
        ]
        + [dma((2, side - 1))] * 8
        + [dma((fs_size - 1,))] * 2,
        compiler_params=pltpu.CompilerParams(
            collective_id=0, has_side_effects=True, vmem_limit_bytes=VMEM_BYTES
        ),
    )(rows_earlier, gate_grad, up_grad, weights, small)
    return gate_sum, up_sum, rows.reshape(tokens, model), small_sum


def contract_last(left, right):
    return lax.dot_general(
        left, right, (((1,), (1,)), ((), ())), preferred_element_type=jnp.float32
    )


def contract_first(left, right):
    return lax.dot_general(
        left, right, (((0,), (0,)), ((), ())), preferred_element_type=jnp.float32
    )


def gather_kernel(
    chips,
    later_ref,
    earlier_ref,
    gate_ref,
    up_ref,
    weights,
    gate_out,
    up_out,
    acc,
    own_sem,
    line_send,
    line_recv,
    pair_send,
    pair_recv,
):
    fs = lax.axis_index("fs")
    fs_size = 2 * chips
    z = fs // 2
    core = lax.rem(fs, 2)
    last = chips - 1
    depth = gate_ref.shape[0]
    tokens = later_ref.shape[0]
    block = math.gcd(tokens, 256)
    parts = (gate_ref, up_ref)
    outs = (gate_out, up_out)
    neighbours = (lax.rem(fs + 2, fs_size), lax.rem(fs + fs_size - 2, fs_size))
    partner = 2 * z + 1 - core

    barrier = pltpu.get_barrier_semaphore()
    for device in neighbours + (partner,):
        pl.semaphore_signal(barrier, inc=1, device_id={"fs": device}, device_id_type=MESH)
    pl.semaphore_wait(barrier, 3)

    def shard(d, half, which):
        return weights.at[half, d, pl.ds(pl.multiple_of(which * depth, depth), depth)]

    def own_copy(half):
        return pltpu.make_async_copy(parts[half], shard(z, half, core), own_sem.at[half])

    def line_copy(way, d, half, own):
        return pltpu.make_async_remote_copy(
            src_ref=parts[half] if own else shard(d, half, core),
            dst_ref=shard(d, half, core),
            send_sem=line_send.at[way, d, half],
            recv_sem=line_recv.at[d, half],
            device_id={"fs": neighbours[way]},
            device_id_type=MESH,
        )

    def pair_copy(d, half, own, which):
        return pltpu.make_async_remote_copy(
            src_ref=parts[half] if own else shard(d, half, which),
            dst_ref=shard(d, half, which),
            send_sem=pair_send.at[d, half],
            recv_sem=pair_recv.at[d, half],
            device_id={"fs": partner},
            device_id_type=MESH,
        )

    def multiply(d, half, first):
        columns = pl.ds(pl.multiple_of(d * 2 * depth, 2 * depth), 2 * depth)
        for micro, rows_ref in enumerate((later_ref, earlier_ref)):

            def body(index, carry):
                rows = pl.ds(pl.multiple_of(index * block, block), block)
                value = jnp.dot(
                    rows_ref[rows, columns],
                    weights[half, d],
                    preferred_element_type=jnp.float32,
                )
                if first:
                    acc[half, micro, rows] = value
                else:
                    acc[half, micro, rows] += value
                return carry

            lax.fori_loop(0, tokens // block, body, 0)

    for half in range(2):

        @pl.when(z < last)
        def _():
            line_copy(0, z, half, True).start()

        @pl.when(z > 0)
        def _():
            line_copy(1, z, half, True).start()

        pair_copy(z, half, True, core).start()
        own_copy(half).start()

    for half in range(2):
        own_copy(half).wait()
        pair_copy(z, half, True, 1 - core).wait_recv()
        multiply(z, half, True)

    def arrive(way, d, half, goes_on):
        line_copy(way, d, half, False).wait_recv()

        @pl.when(goes_on)
        def _():
            line_copy(way, d, half, False).start()

        pair_copy(d, half, False, core).start()

    def use(d, half):
        pair_copy(d, half, False, 1 - core).wait_recv()
        multiply(d, half, False)

    for s in range(1, chips):
        for half in range(2):

            @pl.when(z - s >= 0)
            def _():
                arrive(0, z - s, half, z < last)

            @pl.when(z + s <= last)
            def _():
                arrive(1, z + s, half, z > 0)

            @pl.when(z - s >= 0)
            def _():
                use(z - s, half)

            @pl.when(z + s <= last)
            def _():
                use(z + s, half)

    for half in range(2):
        for micro in range(2):

            def body(index, carry):
                rows = pl.ds(pl.multiple_of(index * block, block), block)
                outs[half][micro, rows] = acc[half, micro, rows].astype(outs[half].dtype)
                return carry

            lax.fori_loop(0, tokens // block, body, 0)

    for half in range(2):
        for d in range(chips):
            pair_copy(d, half, False, core).wait_send()

            @pl.when(jnp.logical_and(d <= z, z < last))
            def _():
                line_copy(0, d, half, False).wait_send()

            @pl.when(jnp.logical_and(d >= z, z > 0))
            def _():
                line_copy(1, d, half, False).wait_send()


def gather_multiply(rows_later, rows_earlier, gate_proj, up_proj):
    chips = lax.axis_size("fs") // 2
    tokens = rows_later.shape[0]
    depth, width = gate_proj.shape
    bf16, dma = jnp.bfloat16, pltpu.SemaphoreType.DMA
    vmem = pl.BlockSpec(memory_space=pltpu.VMEM)
    weights, gate_pre, up_value = pl.pallas_call(
        functools.partial(gather_kernel, chips),
        out_shape=(
            jax.ShapeDtypeStruct((2, chips, 2 * depth, width), bf16),
            jax.ShapeDtypeStruct((2, tokens, width), bf16),
            jax.ShapeDtypeStruct((2, tokens, width), bf16),
        ),
        in_specs=[vmem] * 4,
        out_specs=(vmem, vmem, vmem),
        scratch_shapes=[
            pltpu.VMEM((2, 2, tokens, width), jnp.float32),
            dma((2,)),
            dma((2, chips, 2)),
            dma((chips, 2)),
            dma((chips, 2)),
            dma((chips, 2)),
        ],
        compiler_params=pltpu.CompilerParams(
            collective_id=1, has_side_effects=True, vmem_limit_bytes=VMEM_BYTES
        ),
    )(rows_later, rows_earlier, gate_proj, up_proj)
    return weights.reshape(2, -1, width), gate_pre, up_value


def middle_kernel(
    gate_ref, up_ref, cotangent_ref, taps_ref, bias_ref, hidden_out, up_out, gate_out, small_out
):
    rows, width = cotangent_ref.shape
    count = taps_ref.shape[0]
    index = lax.broadcasted_iota(jnp.int32, (rows, width), 0)

    def down(values, distance):
        if distance == 0:
            return values
        return jnp.where(index >= distance, pltpu.roll(values, distance, 0), 0.0)

    def up(values, distance):
        if distance == 0:
            return values
        moved = pltpu.roll(values, rows - distance, 0)
        return jnp.where(index < rows - distance, moved, 0.0)

    taps = [taps_ref[k : k + 1, :] for k in range(count)]
    for micro in range(2):
        gate = gate_ref[micro].astype(jnp.float32)
        value = up_ref[micro].astype(jnp.float32)
        shifted = [down(gate, count - 1 - k) for k in range(count)]
        mixed = bias_ref[...] + taps[0] * shifted[0]
        for k in range(1, count):
            mixed += taps[k] * shifted[k]
        sig = jax.nn.sigmoid(mixed)
        activated = mixed * sig
        if micro == 0:
            hidden_out[...] = (activated * value).astype(hidden_out.dtype)
            continue
        cotangent = cotangent_ref[...].astype(jnp.float32)
        up_out[...] = (cotangent * activated).astype(up_out.dtype)
        mixed_grad = cotangent * value * sig * (1.0 + mixed * (1.0 - sig))
        total = taps[count - 1] * mixed_grad
        for k in range(count - 1):
            total += taps[k] * up(mixed_grad, count - 1 - k)
        gate_out[...] = total.astype(gate_out.dtype)
        small_out[...] = jnp.zeros_like(small_out)
        for k in range(count):
            small_out[k : k + 1, :] = jnp.sum(mixed_grad * shifted[k], axis=0, keepdims=True)
        small_out[count : count + 1, :] = jnp.sum(mixed_grad, axis=0, keepdims=True)


def middle(gate_pre, up_value, out_cotangent, conv_taps, conv_bias):
    rows, width = out_cotangent.shape
    count = conv_taps.shape[0]
    small_rows = count + 1 + -(count + 1) % 8
    block = math.gcd(width, 128)

    def columns(height):
        return pl.BlockSpec((height, block), lambda i: (0, i))

    pair = pl.BlockSpec((2, rows, block), lambda i: (0, 0, i))
    return pl.pallas_call(
        middle_kernel,
        grid=(width // block,),
        out_shape=(
            jax.ShapeDtypeStruct((rows, width), jnp.bfloat16),
            jax.ShapeDtypeStruct((rows, width), jnp.bfloat16),
            jax.ShapeDtypeStruct((rows, width), jnp.bfloat16),
            jax.ShapeDtypeStruct((small_rows, width), jnp.float32),
        ),
        in_specs=[pair, pair, columns(rows), columns(count), columns(1)],
        out_specs=(columns(rows), columns(rows), columns(rows), columns(small_rows)),
    )(gate_pre, up_value, out_cotangent, conv_taps, conv_bias[None])


def on_device(
    rows_later,
    rows_earlier,
    out_cotangent,
    gate_proj,
    up_proj,
    conv_taps,
    conv_bias,
    gate_grad_sum,
    up_grad_sum,
    taps_grad_sum,
    bias_grad_sum,
):
    seq_len = rows_later.shape[0]
    pieces, gate_pre, up_value = gather_multiply(rows_later, rows_earlier, gate_proj, up_proj)
    grad_scale = lax.rsqrt(jnp.asarray(seq_len * lax.axis_size("fs"), jnp.float32))
    hidden_later, up_grad, gate_grad, small = middle(
        gate_pre, up_value, out_cotangent, conv_taps, conv_bias
    )
    taps = conv_taps.shape[0]
    gate_summed, up_summed, input_grad, small_sum = reduce_all(
        rows_earlier, gate_grad, up_grad, pieces, small
    )
    tap_total, bias_total = small_sum[:taps], small_sum[taps]
    gate_grad_out = gate_grad_sum + grad_scale * gate_summed
    up_grad_out = up_grad_sum + grad_scale * up_summed
    taps_grad_out = taps_grad_sum + grad_scale * tap_total
    bias_grad_out = bias_grad_sum + grad_scale * bias_total
    return (hidden_later, input_grad, gate_grad_out, up_grad_out, taps_grad_out, bias_grad_out)


def solution(mesh):
    placed = (
        P("fs", None),
        P("fs", None),
        P("fs", "tp"),
        P("fs", "tp"),
        P("fs", "tp"),
        P(None, "tp"),
        P("tp"),
        P("fs", "tp"),
        P("fs", "tp"),
        P(None, "tp"),
        P("tp"),
    )
    return jax.shard_map(
        on_device,
        mesh=mesh,
        in_specs=placed,
        out_specs=(
            P("fs", "tp"),
            P("fs", None),
            P("fs", "tp"),
            P("fs", "tp"),
            P(None, "tp"),
            P("tp"),
        ),
        check_vma=False,
    )
```

profile of v0, /device:TPU:0, one launch (start us, length us, event | category | flops | bytes accessed | tf_op | source)
XLA Modules:
  0.0 190.7 jit_solution(18250954478440525171)
XLA Ops:
  0.6 84.8 %shard_map.154 = (bf16[2,4,512,1024]{3,2,1,0:T(8,128)(2,1)}, bf16[2,768,1024]{2,1,0:T(8,128)(2,1)}, bf16[2,768,1024]{2,1,0:T(8,128)(2,1)}) custom-call(bf16[768,2048]{1,0:T(8,128)(2,1)} %later_ref.1, bf16[768,2048]{1,0:T(8,128)(2,1)} %earlier_ref.3, bf16[256,1024]{1,0:T(8,128)(2,1)} %gate_ref.1, bf16[256,1024]{1,0:T(8,128)(2,1)} %up_ref.1), custom_call_target="tpu_custom_call" | custom-call | tf_op jit(solution)/shard_map/pallas_call | solution.py:578
  85.5 9.8 %shard_map.155 = (bf16[768,1024]{1,0:T(8,128)(2,1)}, bf16[768,1024]{1,0:T(8,128)(2,1)}, bf16[768,1024]{1,0:T(8,128)(2,1)}, f32[8,1024]{1,0:T(8,128)}) custom-call(bf16[2,768,1024]{2,1,0:T(8,128)(2,1)} %get-tuple-element.17.gate_ref, bf16[2,768,1024]{2,1,0:T(8,128)(2,1)} %get-tuple-element.18.up_ref, bf16[768,1024]{1,0:T(8,128)(2,1)} %cotangent_ref.1, ...), custom_call_target="tpu_custom_call" | custom-call | tf_op jit(solution)/shard_map/pallas_call | solution.py:656
  95.3 0.0 copy-start.3
  95.3 0.0 copy-start.4
  95.3 0.0 copy-start.1
  95.3 0.0 copy-start.2
  95.3 87.3 %shard_map.156 = (f32[256,1024]{1,0:T(8,128)}, f32[256,1024]{1,0:T(8,128)}, bf16[2,2,2,96,2048]{4,3,2,1,0:T(8,128)(2,1)}, f32[8,1024]{1,0:T(8,128)}) custom-call(bf16[768,2048]{1,0:T(8,128)(2,1)} %earlier_ref.3, bf16[768,1024]{1,0:T(8,128)(2,1)} %get-tuple-element.20.gate_grad_ref, bf16[768,1024]{1,0:T(8,128)(2,1)} %get-tuple-element.21.up_grad_ref, ...), custom_call_target="tpu_custom_call" | custom-call | tf_op jit(solution)/shard_map/pallas_call | solution.py:374
  182.7 0.8 slice_multiply_fusion
  183.4 0.0 copy-done.3
  183.4 1.4 multiply_add_fusion.2
  184.8 0.0 copy-done.4
  184.8 0.6 add.15
  185.4 0.0 copy-done.1
  185.4 0.0 copy-done.2
  185.4 0.0 copy-start
  185.4 3.6 %multiply_add_fusion = (f32[256,1024]{1,0:T(8,128)}, f32[256,1024]{1,0:T(8,128)}) fusion(f32[256,1024]{1,0:T(8,128)S(1)} %copy-done.1, f32[256,1024]{1,0:T(8,128)} %get-tuple-element.26, f32[256,1024]{1,0:T(8,128)S(1)} %copy-done.2, f32[256,1024]{1,0:T(8,128)} %get-tuple-element.25), kind=kLoop, calls=%fused_computation | loop fusion | flops 1048576 | bytes 6291456 | tf_op jit(solution)/shard_map/add | solution.py:695
  189.0 0.0 copy-done
  189.0 1.7 copy.18
Async XLA Ops:
  95.3 88.1 %copy-start.3 = (f32[3,1024]{1,0:T(4,128)S(1)}, f32[3,1024]{1,0:T(4,128)}, u32[]{:S(2)}) copy-start(f32[3,1024]{1,0:T(4,128)} %param.20) | copy-start | bytes 36868
  95.3 89.5 %copy-start.4 = (f32[1024]{0:T(1024)S(1)}, f32[1024]{0:T(1024)}, u32[]{:S(2)}) copy-start(f32[1024]{0:T(1024)} %param.21) | copy-start | bytes 12292
  95.3 90.1 %copy-start.1 = (f32[256,1024]{1,0:T(8,128)S(1)}, f32[256,1024]{1,0:T(8,128)}, u32[]{:S(2)}) copy-start(f32[256,1024]{1,0:T(8,128)} %param.19) | copy-start | bytes 3145732
  95.3 90.1 %copy-start.2 = (f32[256,1024]{1,0:T(8,128)S(1)}, f32[256,1024]{1,0:T(8,128)}, u32[]{:S(2)}) copy-start(f32[256,1024]{1,0:T(8,128)} %param.18) | copy-start | bytes 3145732
  185.4 3.6 %copy-start = (bf16[2,2,2,96,2048]{4,3,2,1,0:T(8,128)(2,1)S(1)}, bf16[2,2,2,96,2048]{4,3,2,1,0:T(8,128)(2,1)}, u32[]{:S(2)}) copy-start(bf16[2,2,2,96,2048]{4,3,2,1,0:T(8,128)(2,1)} %get-tuple-element.24) | copy-start | bytes 9437188
where the time goes:
time: 191 us
  Pallas kernels  182 us (95%)
  other arithmetic  6.35 us (3%)
    pallas_call x1, Pallas kernels, reduce_all(): pl.pallas_call(functools.partial(reduce_kernel, chips, side), out_shape=(...  87.3 us
    pallas_call x1, Pallas kernels, gather_multiply(): pl.pallas_call(functools.partial(gather_kernel, chips), out_shape=(jax.Sh...  84.8 us
    pallas_call x1, Pallas kernels, middle(): pl.pallas_call(middle_kernel, grid=(width // block,), out_shape=(jax.Shap...  9.82 us

commit v1 on v0

v1 whole, which is shorter than its diff:
```python
import functools
import math

import jax
import jax.numpy as jnp
from jax import lax
from jax.experimental import pallas as pl
from jax.experimental.pallas import tpu as pltpu
from jax.sharding import PartitionSpec as P

MESH = pl.DeviceIdType.MESH
VMEM_BYTES = 62 * 1024 * 1024
F32, BF16 = jnp.float32, jnp.bfloat16


def contract_last(left, right):
    return lax.dot_general(
        left, right, (((1,), (1,)), ((), ())), preferred_element_type=jnp.float32
    )


def down(values, distance):
    if distance == 0:
        return values
    index = lax.broadcasted_iota(jnp.int32, values.shape, 0)
    return jnp.where(index >= distance, pltpu.roll(values, distance, 0), 0.0)


def up(values, distance):
    if distance == 0:
        return values
    rows = values.shape[0]
    index = lax.broadcasted_iota(jnp.int32, values.shape, 0)
    return jnp.where(index < rows - distance, pltpu.roll(values, rows - distance, 0), 0.0)


class Sizes:
    def __init__(self, fs_size, tp_size, tokens, model, depth, width, taps):
        self.fs_size = fs_size
        self.chips = fs_size // 2
        self.side = math.isqrt(tp_size)
        self.tokens, self.model, self.depth, self.width = tokens, model, depth, width
        self.w = math.gcd(width, 128)
        self.n = width // self.w
        self.taps = taps
        block = tokens // (2 * self.side)
        self.q = max(q for q in (1, 2, 3, 4) if block % (16 * q) == 0)
        self.r = block // self.q
        self.scale = 1.0 / math.sqrt(tokens * fs_size)


def kernel(
    sizes,
    later_hbm,
    earlier_hbm,
    cot_hbm,
    gate_hbm,
    up_hbm,
    gate_sum_hbm,
    up_sum_hbm,
    taps_ref,
    bias_ref,
    taps_sum_ref,
    bias_sum_ref,
    hidden_hbm,
    rows_hbm,
    gate_out_hbm,
    up_out_hbm,
    taps_out,
    bias_out,
    later_v,
    earlier_v,
    earlier_t,
    cot_v,
    weights,
    pre,
    grads,
    hidden_v,
    acc,
    own_t,
    out_t,
    pair_t,
    ring,
    sums,
    rows_s,
    first_in,
    second_in,
    rows_buf,
    small_v,
    small_buf,
    weight_load,
    rows_load,
    cot_load,
    sum_load,
    sum_store,
    hidden_store,
    rows_store,
    line_send,
    line_recv,
    pair_send,
    pair_recv,
    term_send,
    term_recv,
    ring_send,
    ring_recv,
    first_send,
    first_recv,
    second_send,
    second_recv,
    third_send,
    third_recv,
    small_send,
    small_recv,
):
    n, w, q, r = sizes.n, sizes.w, sizes.q, sizes.r
    chips, side, depth = sizes.chips, sizes.side, sizes.depth
    fs_size, tokens, model = sizes.fs_size, sizes.tokens, sizes.model
    count = sizes.taps
    last = chips - 1
    fs = lax.axis_index("fs")
    tp = lax.axis_index("tp")
    z = fs // 2
    core = lax.rem(fs, 2)
    partner = 2 * z + 1 - core
    neighbours = (lax.rem(fs + 2, fs_size), lax.rem(fs + fs_size - 2, fs_size))
    ty = tp // side
    tx = lax.rem(tp, side)
    firsts = (tx, ty)
    seconds = (ty, tx)

    def first_peer(half, k):
        peer = lax.rem(firsts[half] + k, side)
        return peer, (ty * side + peer if half == 0 else peer * side + tx)

    def second_peer(half, k):
        peer = lax.rem(seconds[half] + k, side)
        return peer, (peer * side + tx if half == 0 else ty * side + peer)

    def columns(c):
        return pl.ds(pl.multiple_of(c * w, w), w)

    def own_rows(which):
        return pl.ds(pl.multiple_of((2 * z + which) * depth, depth), depth)

    def load_weight(c, which):
        source = (gate_hbm, up_hbm)[which]
        return pltpu.make_async_copy(
            source.at[:, columns(c)],
            weights.at[c, own_rows(core), pl.ds(which * w, w)],
            weight_load.at[c, which],
        )

    def load_rows(which):
        return pltpu.make_async_copy(
            (later_hbm, earlier_hbm)[which], (later_v, earlier_v)[which], rows_load.at[which]
        )

    def load_cot(c):
        return pltpu.make_async_copy(cot_hbm.at[:, columns(c)], cot_v.at[c], cot_load.at[c])

    def load_sum(c, which):
        source = (gate_sum_hbm, up_sum_hbm)[which]
        return pltpu.make_async_copy(
            source.at[:, columns(c)], sums.at[c, :, pl.ds(which * w, w)], sum_load.at[c, which]
        )

    def store_sum(c, which):
        target = (gate_out_hbm, up_out_hbm)[which]
        return pltpu.make_async_copy(
            sums.at[c, :, pl.ds(which * w, w)], target.at[:, columns(c)], sum_store.at[c, which]
        )

    def store_hidden(c):
        return pltpu.make_async_copy(
            hidden_v.at[c], hidden_hbm.at[:, columns(c)], hidden_store.at[c]
        )

    def piece(half, i, p):
        start = ((half * side + i) * q + p) * r
        return pl.ds(pl.multiple_of(start, r), r)

    def store_rows(half, i, p):
        block = piece(half, i, p)
        return pltpu.make_async_copy(
            rows_buf.at[block], rows_hbm.at[block], rows_store.at[half, i, p]
        )

    def remote(source, target, send, recv, device):
        return pltpu.make_async_remote_copy(
            src_ref=source,
            dst_ref=target,
            send_sem=send,
            recv_sem=recv,
            device_id=device,
            device_id_type=MESH,
        )

    def shard(o, which, c):
        return weights.at[c, pl.ds(pl.multiple_of((2 * o + which) * depth, depth), depth)]

    def line_copy(way, o, c):
        ref = shard(o, core, c)
        return remote(
            ref, ref, line_send.at[way, c, o], line_recv.at[c, o], {"fs": neighbours[way]}
        )

    def pair_copy(o, which, c):
        ref = shard(o, which, c)
        return remote(ref, ref, pair_send.at[c, o], pair_recv.at[c, o], {"fs": partner})

    def term_copy(c):
        return remote(
            out_t.at[lax.rem(c, 2)],
            pair_t.at[c],
            term_send.at[c],
            term_recv.at[c],
            {"fs": partner},
        )

    def ring_slot(way, c, d):
        return ring.at[way, c, d - 1 if way == 0 else d]

    def ring_copy(way, c, d):
        at = (way, c, d - 1 if way == 0 else d)
        slot = ring.at[at]
        return remote(slot, slot, ring_send.at[at], ring_recv.at[at], {"fs": neighbours[way]})

    def first_copy(half, k, p):
        peer, device = first_peer(half, k)
        at = (half, k - 1, p)
        return remote(
            rows_s.at[piece(half, peer, p)],
            first_in.at[at],
            first_send.at[at],
            first_recv.at[at],
            {"tp": device},
        )

    def second_copy(half, k, p, position):
        _, device = second_peer(half, k)
        slot = second_in.at[half, position, p]
        at = (half, k - 1, p)
        return remote(slot, slot, second_send.at[at], second_recv.at[at], {"tp": device})

    def third_copy(half, k, p, shown):
        _, device = first_peer(half, k)
        block = rows_buf.at[piece(half, shown, p)]
        at = (half, k - 1, p)
        return remote(block, block, third_send.at[at], third_recv.at[at], {"tp": device})

    def small_copy(k, slot):
        return remote(
            small_v,
            small_buf.at[slot],
            small_send.at[k - 1],
            small_recv.at[k - 1],
            {"fs": lax.rem(fs + k, fs_size)},
        )

    for c in range(n):
        load_weight(c, 0).start()
        load_weight(c, 1).start()

    barrier = pltpu.get_barrier_semaphore()
    for k in range(1, fs_size):
        pl.semaphore_signal(
            barrier, inc=1, device_id={"fs": lax.rem(fs + k, fs_size)}, device_id_type=MESH
        )
    for half in range(2):
        for k in range(1, side):
            pl.semaphore_signal(
                barrier, inc=1, device_id={"tp": first_peer(half, k)[1]}, device_id_type=MESH
            )

    load_rows(1).start()
    for c in range(n):
        load_cot(c).start()
    load_rows(0).start()
    for c in range(n):
        load_sum(c, 0).start()
        load_sum(c, 1).start()

    pl.semaphore_wait(barrier, fs_size - 1 + 2 * (side - 1))

    block = math.gcd(tokens, 256)
    wide = math.gcd(model, 512)

    def forward(rows_v, c):
        def body(index, carry):
            rows = pl.ds(pl.multiple_of(index * block, block), block)
            value = jnp.dot(rows_v[rows, :], weights[c], preferred_element_type=F32)
            pre[rows, :] = value.astype(BF16)
            return carry

        lax.fori_loop(0, tokens // block, body, 0)

    def mixing(c):
        gate = pre[:, :w].astype(F32)
        value = pre[:, w:].astype(F32)
        taps = [taps_ref[k : k + 1, columns(c)] for k in range(count)]
        shifted = [down(gate, count - 1 - k) for k in range(count)]
        mixed = bias_ref[:, columns(c)] + taps[0] * shifted[0]
        for k in range(1, count):
            mixed += taps[k] * shifted[k]
        sig = jax.nn.sigmoid(mixed)
        return value, taps, shifted, mixed, sig

    def middle_later(c):
        value, _, _, mixed, sig = mixing(c)
        hidden_v[c] = (mixed * sig * value).astype(BF16)

    def middle_earlier(c):
        value, taps, shifted, mixed, sig = mixing(c)
        cot = cot_v[c].astype(F32)
        grads[:, w:] = (cot * (mixed * sig)).astype(BF16)
        mixed_grad = cot * value * sig * (1.0 + mixed * (1.0 - sig))
        total = taps[count - 1] * mixed_grad
        for k in range(count - 1):
            total += taps[k] * up(mixed_grad, count - 1 - k)
        grads[:, :w] = total.astype(BF16)
        for k in range(count):
            small_v[c, k : k + 1, :] = jnp.sum(mixed_grad * shifted[k], axis=0, keepdims=True)
        small_v[c, count : count + 1, :] = jnp.sum(mixed_grad, axis=0, keepdims=True)

    def add_rows(c):
        def body(index, carry):
            cols = pl.ds(pl.multiple_of(index * wide, wide), wide)
            value = contract_last(grads[...], weights[c, cols, :])
            acc[:, cols] += value
            return carry

        lax.fori_loop(0, model // wide, body, 0)

    def last_rows(c):
        def body(index, carry):
            cols = pl.ds(pl.multiple_of(index * wide, wide), wide)
            value = contract_last(grads[...], weights[c, cols, :])
            rows_s[:, cols] = (acc[:, cols] + value).astype(BF16)
            return carry

        lax.fori_loop(0, model // wide, body, 0)
        for p in range(q):
            for k in range(1, side):
                for half in range(2):
                    first_copy(half, k, p).start()

    def make_terms(c):
        @pl.when(c >= 2)
        def _():
            term_copy(c - 2).wait_send()

        def fill(target, which):
            def body(d, carry):
                rows = pl.ds(pl.multiple_of((2 * d + which) * depth, depth), depth)
                value = jnp.dot(earlier_t[rows, :], grads[...], preferred_element_type=F32)
                target[d] = value.astype(BF16)
                return carry

            lax.fori_loop(0, chips, body, 0)

        fill(out_t.at[lax.rem(c, 2)], 1 - core)
        term_copy(c).start()
        fill(own_t.at[c], core)

    def transpose_rows():
        acc[...] = jnp.zeros_like(acc)
        small_v[...] = jnp.zeros_like(small_v)
        step = math.gcd(model, 256)

        def body(index, carry):
            cols = pl.ds(pl.multiple_of(index * step, step), step)
            earlier_t[cols, :] = earlier_v[:, cols].T
            return carry

        lax.fori_loop(0, model // step, body, 0)

    def compute(c):
        @pl.when(c == 0)
        def _():
            load_rows(1).wait()
            transpose_rows()

        for o in range(chips):
            pair_copy(o, 1 - core, c).wait_recv()
        forward(earlier_v, c)
        load_cot(c).wait()
        middle_earlier(c)

        @pl.when(c < n - 1)
        def _():
            add_rows(c)

        @pl.when(c == n - 1)
        def _():
            last_rows(c)
            for k in range(1, fs_size):
                small_copy(k, fs).start()

        make_terms(c)

        @pl.when(c == 0)
        def _():
            load_rows(0).wait()

        forward(later_v, c)
        middle_later(c)
        store_hidden(c).start()
        term_copy(c).wait_recv()

    def arrive(way, o, c, goes_on):
        line_copy(way, o, c).wait_recv()

        @pl.when(goes_on)
        def _():
            line_copy(way, o, c).start()

        pair_copy(o, core, c).start()

    def push(way, c, d, first_on_line):
        slot = ring_slot(way, c, d)

        @pl.when(first_on_line)
        def _():
            slot[...] = (own_t[c, d].astype(F32) + pair_t[c, d].astype(F32)).astype(BF16)

        @pl.when(jnp.logical_not(first_on_line))
        def _():
            ring_copy(way, c, d).wait_recv()
            total = own_t[c, d].astype(F32) + pair_t[c, d].astype(F32) + slot[...].astype(F32)
            slot[...] = total.astype(BF16)

        ring_copy(way, c, d).start()

    def push_up(c, carry):
        for d in range(last, 0, -1):

            @pl.when(d > z)
            def _():
                push(0, c, d, z == 0)

        return carry

    def push_down(c, carry):
        for d in range(last):

            @pl.when(d < z)
            def _():
                push(1, c, d, z == last)

        return carry

    def finish_sum(c, carry):
        load_sum(c, 0).wait()
        load_sum(c, 1).wait()
        base = own_t[c, z].astype(F32) + pair_t[c, z].astype(F32)
        sums[c] += sizes.scale * base

        @pl.when(z > 0)
        def _():
            ring_copy(0, c, z).wait_recv()
            sums[c] += sizes.scale * ring_slot(0, c, z)[...].astype(F32)

        @pl.when(z < last)
        def _():
            ring_copy(1, c, z).wait_recv()
            sums[c] += sizes.scale * ring_slot(1, c, z)[...].astype(F32)

        store_sum(c, 0).start()
        store_sum(c, 1).start()
        return carry

    far = jnp.maximum(z, last - z)
    lag = max(n // 2, 1)

    def pushed(i, hops):
        return jnp.clip(i + 1 - lag * hops + jnp.maximum(i - (n - 1), 0), 0, n)

    def exchange(j):
        for half in range(2):

            @pl.when(jnp.logical_and(j >= 1, j <= q))
            def _():
                p = j - 1
                total = rows_s[piece(half, firsts[half], p), :].astype(F32)
                for k in range(1, side):
                    first_copy(half, k, p).wait_recv()
                    total += first_in[half, k - 1, p].astype(F32)
                second_in[half, seconds[half], p] = total.astype(BF16)
                for k in range(1, side):
                    second_copy(half, k, p, seconds[half]).start()

            @pl.when(jnp.logical_and(j > q, j <= 2 * q))
            def _():
                p = j - 1 - q
                for k in range(1, side):
                    position = lax.rem(seconds[half] + side - k, side)
                    second_copy(half, k, p, position).wait_recv()
                total = second_in[half, 0, p].astype(F32)
                for position in range(1, side):
                    total += second_in[half, position, p].astype(F32)
                rows_buf[piece(half, firsts[half], p), :] = total.astype(BF16)
                for k in range(1, side):
                    third_copy(half, k, p, firsts[half]).start()
                store_rows(half, firsts[half], p).start()

            @pl.when(jnp.logical_and(j > 2 * q, j <= 3 * q))
            def _():
                p = j - 1 - 2 * q
                for k in range(1, side):
                    source = lax.rem(firsts[half] + side - k, side)
                    third_copy(half, k, p, source).wait_recv()
                    store_rows(half, source, p).start()

    def step(s, carry):
        i = s - far

        @pl.when(s < n)
        def _():
            load_weight(s, 0).wait()
            load_weight(s, 1).wait()

            @pl.when(z < last)
            def _():
                line_copy(0, z, s).start()

            @pl.when(z > 0)
            def _():
                line_copy(1, z, s).start()

            pair_copy(z, core, s).start()

        for k in range(1, chips):
            c = s - k
            inside = jnp.logical_and(c >= 0, c < n)

            @pl.when(jnp.logical_and(inside, z - k >= 0))
            def _():
                arrive(0, z - k, c, z < last)

            @pl.when(jnp.logical_and(inside, z + k <= last))
            def _():
                arrive(1, z + k, c, z > 0)

        @pl.when(jnp.logical_and(i >= 0, i < n))
        def _():
            compute(i)

        lax.fori_loop(pushed(i - 1, z), pushed(i, z), push_up, 0)
        lax.fori_loop(pushed(i - 1, last - z), pushed(i, last - z), push_down, 0)
        lax.fori_loop(pushed(i - 1, far), pushed(i, far), finish_sum, 0)
        exchange(i - (n - 1))
        return carry

    end = max(n - 1 + 3 * q, n - 1 + -(-lag * last // 2))
    lax.fori_loop(0, end + last + 1, step, 0)

    small_buf[fs] = small_v[...]
    for k in range(1, fs_size):
        small_copy(k, lax.rem(fs + fs_size - k, fs_size)).wait_recv()
    for c in range(n):
        total = small_buf[0, c]
        for source in range(1, fs_size):
            total += small_buf[source, c]
        total = sizes.scale * total
        cols = slice(c * w, (c + 1) * w)
        taps_out[:, cols] = taps_sum_ref[:, cols] + total[:count]
        bias_out[:, cols] = bias_sum_ref[:, cols] + total[count : count + 1]

    for k in range(1, fs_size):
        small_copy(k, fs).wait_send()

    def drain(c, carry):
        def over_chips(d, inner):
            pair_copy(d, core, c).wait_send()

            @pl.when(jnp.logical_and(d <= z, z < last))
            def _():
                line_copy(0, d, c).wait_send()

            @pl.when(jnp.logical_and(d >= z, z > 0))
            def _():
                line_copy(1, d, c).wait_send()

            @pl.when(d > z)
            def _():
                ring_copy(0, c, d).wait_send()

            @pl.when(d < z)
            def _():
                ring_copy(1, c, d).wait_send()

            return inner

        lax.fori_loop(0, chips, over_chips, 0)

        @pl.when(c >= n - 2)
        def _():
            term_copy(c).wait_send()

        store_hidden(c).wait()
        store_sum(c, 0).wait()
        store_sum(c, 1).wait()
        return carry

    lax.fori_loop(0, n, drain, 0)
    for half in range(2):
        for p in range(q):
            for k in range(1, side):
                first_copy(half, k, p).wait_send()
                second_copy(half, k, p, seconds[half]).wait_send()
                third_copy(half, k, p, firsts[half]).wait_send()
            for i in range(side):
                store_rows(half, i, p).wait()


def on_device(
    rows_later,
    rows_earlier,
    out_cotangent,
    gate_proj,
    up_proj,
    conv_taps,
    conv_bias,
    gate_grad_sum,
    up_grad_sum,
    taps_grad_sum,
    bias_grad_sum,
):
    tokens, model = rows_later.shape
    depth, width = gate_proj.shape
    taps = conv_taps.shape[0]
    sizes = Sizes(
        lax.axis_size("fs"), lax.axis_size("tp"), tokens, model, depth, width, taps
    )
    n, w, q, r = sizes.n, sizes.w, sizes.q, sizes.r
    chips, side, fs_size = sizes.chips, sizes.side, sizes.fs_size
    dma = pltpu.SemaphoreType.DMA
    whole = pl.BlockSpec(memory_space=pltpu.VMEM)
    far = pl.BlockSpec(memory_space=pl.ANY)
    links = max(side - 1, 1)
    outs = pl.pallas_call(
        functools.partial(kernel, sizes),
        out_shape=(
            jax.ShapeDtypeStruct((tokens, width), BF16),
            jax.ShapeDtypeStruct((tokens, model), BF16),
            jax.ShapeDtypeStruct((depth, width), F32),
            jax.ShapeDtypeStruct((depth, width), F32),
            jax.ShapeDtypeStruct((taps, width), F32),
            jax.ShapeDtypeStruct((1, width), F32),
        ),
        in_specs=[far] * 7 + [whole] * 4,
        out_specs=(far, far, far, far, whole, whole),
        scratch_shapes=[
            pltpu.VMEM((tokens, model), BF16),
            pltpu.VMEM((tokens, model), BF16),
            pltpu.VMEM((model, tokens), BF16),
            pltpu.VMEM((n, tokens, w), BF16),
            pltpu.VMEM((n, model, 2 * w), BF16),
            pltpu.VMEM((tokens, 2 * w), BF16),
            pltpu.VMEM((tokens, 2 * w), BF16),
            pltpu.VMEM((n, tokens, w), BF16),
            pltpu.VMEM((tokens, model), F32),
            pltpu.VMEM((n, chips, depth, 2 * w), BF16),
            pltpu.VMEM((2, chips, depth, 2 * w), BF16),
            pltpu.VMEM((n, chips, depth, 2 * w), BF16),
            pltpu.VMEM((2, n, max(chips - 1, 1), depth, 2 * w), BF16),
            pltpu.VMEM((n, depth, 2 * w), F32),
            pltpu.VMEM((tokens, model), BF16),
            pltpu.VMEM((2, links, q, r, model), BF16),
            pltpu.VMEM((2, side, q, r, model), BF16),
            pltpu.VMEM((tokens, model), BF16),
            pltpu.VMEM((n, 8 * -(-(taps + 1) // 8), w), F32),
            pltpu.VMEM((fs_size, n, 8 * -(-(taps + 1) // 8), w), F32),
            dma((n, 2)),
            dma((2,)),
            dma((n,)),
            dma((n, 2)),
            dma((n, 2)),
            dma((n,)),
            dma((2, side, q)),
            dma((2, n, chips)),
            dma((n, chips)),
            dma((n, chips)),
            dma((n, chips)),
            dma((n,)),
            dma((n,)),
            dma((2, n, max(chips - 1, 1))),
            dma((2, n, max(chips - 1, 1))),
        ]
        + [dma((2, links, q))] * 6
        + [dma((fs_size - 1,))] * 2,
        compiler_params=pltpu.CompilerParams(
            collective_id=0, has_side_effects=True, vmem_limit_bytes=VMEM_BYTES
        ),
    )(
        rows_later,
        rows_earlier,
        out_cotangent,
        gate_proj,
        up_proj,
        gate_grad_sum,
        up_grad_sum,
        conv_taps,
        conv_bias[None],
        taps_grad_sum,
        bias_grad_sum[None],
    )
    hidden_later, input_grad, gate_grad_out, up_grad_out, taps_grad_out, bias_grad_out = outs
    return (
        hidden_later,
        input_grad,
        gate_grad_out,
        up_grad_out,
        taps_grad_out,
        bias_grad_out[0],
    )


def solution(mesh):
    placed = (
        P("fs", None),
        P("fs", None),
        P("fs", "tp"),
        P("fs", "tp"),
        P("fs", "tp"),
        P(None, "tp"),
        P("tp"),
        P("fs", "tp"),
        P("fs", "tp"),
        P(None, "tp"),
        P("tp"),
    )
    return jax.shard_map(
        on_device,
        mesh=mesh,
        in_specs=placed,
        out_specs=(
            P("fs", "tp"),
            P("fs", None),
            P("fs", "tp"),
            P("fs", "tp"),
            P(None, "tp"),
            P("tp"),
        ),
        check_vma=False,
    )
```

time: 191 us -> 166 us (0.87)
  Pallas kernels: 182 us -> 158 us
  other arithmetic: 6.35 us -> 0 us
  local copies, waits for them, and re-layouts: 1.69 us -> 7.93 us
    pallas_call x3 -> x1, Pallas kernels: 182 us -> 158 us  [on_device(): pl.pallas_call(functools.partial(kernel, sizes), out_shape=(jax.ShapeDtyp...]
    unnamed x11 -> x16, local copies, waits for them, and re-layouts: 1.69 us -> 7.93 us
    add x3 -> x0, other arithmetic: 5.59 us -> none  [the longest x1 3.62 us: on_device(): up_grad_out = up_grad_sum + grad_scale * up_summed]
where the time goes in v1:
time: 166 us
  Pallas kernels  158 us (95%)
  local copies, waits for them, and re-layouts  7.93 us (5%)
    pallas_call x1, Pallas kernels, on_device(): pl.pallas_call(functools.partial(kernel, sizes), out_shape=(jax.ShapeDtyp...  158 us
    unnamed x16, local copies, waits for them, and re-layouts  7.93 us

profile of v1, /device:TPU:0, one launch (start us, length us, event | category | flops | bytes accessed | tf_op | source)
XLA Modules:
  0.0 166.1 jit_solution(7652113339170549410)
XLA Ops:
  0.6 157.5 %shard_map.154 = (bf16[768,1024]{1,0:T(8,128)(2,1)}, bf16[768,2048]{1,0:T(8,128)(2,1)}, f32[256,1024]{1,0:T(8,128)}, f32[256,1024]{1,0:T(8,128)}, f32[3,1024]{1,0:T(4,128)}, /*index=5*/f32[1,1024]{1,0:T(1,128)}) custom-call(bf16[768,2048]{1,0:T(8,128)(2,1)} %later_hbm.1, bf16[768,2048]{1,0:T(8,128)(2,1)} %earlier_hbm.1, bf16[768,1024]{1,0:T(8,128)(2,1)} %cot_hbm.1, ...), custom_call_target="tpu_custom_call" | custom-call | tf_op jit(solution)/shard_map/pallas_call | solution.py:641
  158.2 0.0 copy-start
  158.2 2.8 %copy.23 = bf16[768,1024]{1,0:T(8,128)(2,1)} copy(bf16[768,1024]{1,0:T(8,128)(2,1)} %get-tuple-element.24) | data formatting | bytes 3145728
  161.0 0.0 copy-done
  161.0 0.0 copy-start.2
  161.0 0.0 copy-start.1
  161.0 1.7 %copy.24 = bf16[768,2048]{1,0:T(8,128)(2,1)} copy(bf16[768,2048]{1,0:T(8,128)(2,1)S(1)} %copy-done) | data formatting | bytes 6291456
  162.7 0.3 copy-done.2
  162.9 0.0 copy-start.3
  163.0 0.0 copy-start.4
  163.0 1.0 copy.25
  163.9 0.0 copy-done.1
  163.9 1.0 copy.26
  164.9 0.0 copy-done.3
  164.9 0.6 copy.27
  165.5 0.0 copy-done.4
  165.5 0.6 copy.28
Async XLA Ops:
  158.2 2.8 %copy-start = (bf16[768,2048]{1,0:T(8,128)(2,1)S(1)}, bf16[768,2048]{1,0:T(8,128)(2,1)}, u32[]{:S(2)}) copy-start(bf16[768,2048]{1,0:T(8,128)(2,1)} %get-tuple-element.25) | copy-start | bytes 9437188
  161.0 2.0 %copy-start.2 = (f32[256,1024]{1,0:T(8,128)S(1)}, f32[256,1024]{1,0:T(8,128)}, u32[]{:S(2)}) copy-start(f32[256,1024]{1,0:T(8,128)} %get-tuple-element.26) | copy-start | bytes 3145732
  161.0 2.9 %copy-start.1 = (f32[256,1024]{1,0:T(8,128)S(1)}, f32[256,1024]{1,0:T(8,128)}, u32[]{:S(2)}) copy-start(f32[256,1024]{1,0:T(8,128)} %get-tuple-element.27) | copy-start | bytes 3145732
  162.9 1.9 %copy-start.3 = (f32[3,1024]{1,0:T(4,128)S(1)}, f32[3,1024]{1,0:T(4,128)}, u32[]{:S(2)}) copy-start(f32[3,1024]{1,0:T(4,128)} %get-tuple-element.28) | copy-start | bytes 36868
  163.0 2.6 %copy-start.4 = (f32[1,1024]{1,0:T(1,128)S(1)}, f32[1,1024]{1,0:T(1,128)}, u32[]{:S(2)}) copy-start(f32[1,1024]{1,0:T(1,128)} %get-tuple-element.17) | copy-start | bytes 12292

commit v2 on v1

--- a/solution.py
+++ b/solution.py
@@ -9,7 +9,8 @@
 from jax.sharding import PartitionSpec as P
 
 MESH = pl.DeviceIdType.MESH
-VMEM_BYTES = 62 * 1024 * 1024
+VMEM_BYTES = 56 * 1024 * 1024
+FORWARD_ROWS = 768
 F32, BF16 = jnp.float32, jnp.bfloat16
 
 
@@ -43,9 +44,10 @@
         self.w = math.gcd(width, 128)
         self.n = width // self.w
         self.taps = taps
-        block = tokens // (2 * self.side)
-        self.q = max(q for q in (1, 2, 3, 4) if block % (16 * q) == 0)
-        self.r = block // self.q
+        self.group = math.gcd(self.n, 2)
+        self.r = tokens // (2 * self.side)
+        self.q = max(q for q in (1, 2, 4) if model % (128 * q) == 0)
+        self.cut = model // self.q
         self.scale = 1.0 / math.sqrt(tokens * fs_size)
 
 
@@ -62,10 +64,10 @@
     bias_ref,
     taps_sum_ref,
     bias_sum_ref,
-    hidden_hbm,
-    rows_hbm,
-    gate_out_hbm,
-    up_out_hbm,
+    hidden_out,
+    rows_out,
+    gate_out,
+    up_out,
     taps_out,
     bias_out,
     later_v,
@@ -75,26 +77,20 @@
     weights,
     pre,
     grads,
-    hidden_v,
     acc,
     own_t,
     out_t,
     pair_t,
     ring,
-    sums,
     rows_s,
     first_in,
     second_in,
-    rows_buf,
     small_v,
     small_buf,
     weight_load,
     rows_load,
     cot_load,
     sum_load,
-    sum_store,
-    hidden_store,
-    rows_store,
     line_send,
     line_recv,
     pair_send,
@@ -112,7 +108,8 @@
     small_send,
     small_recv,
 ):
-    n, w, q, r = sizes.n, sizes.w, sizes.q, sizes.r
+    n, w, q, r, cut = sizes.n, sizes.w, sizes.q, sizes.r, sizes.cut
+    group = sizes.group
     chips, side, depth = sizes.chips, sizes.side, sizes.depth
     fs_size, tokens, model = sizes.fs_size, sizes.tokens, sizes.model
     count = sizes.taps
@@ -158,32 +155,14 @@
     def load_cot(c):
         return pltpu.make_async_copy(cot_hbm.at[:, columns(c)], cot_v.at[c], cot_load.at[c])
 
-    def load_sum(c, which):
-        source = (gate_sum_hbm, up_sum_hbm)[which]
+    def load_sum(which):
         return pltpu.make_async_copy(
-            source.at[:, columns(c)], sums.at[c, :, pl.ds(which * w, w)], sum_load.at[c, which]
-        )
-
-    def store_sum(c, which):
-        target = (gate_out_hbm, up_out_hbm)[which]
-        return pltpu.make_async_copy(
-            sums.at[c, :, pl.ds(which * w, w)], target.at[:, columns(c)], sum_store.at[c, which]
-        )
-
-    def store_hidden(c):
-        return pltpu.make_async_copy(
-            hidden_v.at[c], hidden_hbm.at[:, columns(c)], hidden_store.at[c]
+            (gate_sum_hbm, up_sum_hbm)[which], (gate_out, up_out)[which], sum_load.at[which]
         )
 
     def piece(half, i, p):
-        start = ((half * side + i) * q + p) * r
-        return pl.ds(pl.multiple_of(start, r), r)
-
-    def store_rows(half, i, p):
-        block = piece(half, i, p)
-        return pltpu.make_async_copy(
-            rows_buf.at[block], rows_hbm.at[block], rows_store.at[half, i, p]
-        )
+        rows = pl.ds(pl.multiple_of((half * side + i) * r, r), r)
+        return rows, pl.ds(pl.multiple_of(p * cut, cut), cut)
 
     def remote(source, target, send, recv, device):
         return pltpu.make_async_remote_copy(
@@ -244,7 +223,7 @@
 
     def third_copy(half, k, p, shown):
         _, device = first_peer(half, k)
-        block = rows_buf.at[piece(half, shown, p)]
+        block = rows_out.at[piece(half, shown, p)]
         at = (half, k - 1, p)
         return remote(block, block, third_send.at[at], third_recv.at[at], {"tp": device})
 
@@ -276,14 +255,12 @@
     for c in range(n):
         load_cot(c).start()
     load_rows(0).start()
-    for c in range(n):
-        load_sum(c, 0).start()
-        load_sum(c, 1).start()
+    load_sum(0).start()
+    load_sum(1).start()
 
     pl.semaphore_wait(barrier, fs_size - 1 + 2 * (side - 1))
 
-    block = math.gcd(tokens, 256)
-    wide = math.gcd(model, 512)
+    block = math.gcd(tokens, FORWARD_ROWS)
 
     def forward(rows_v, c):
         def body(index, carry):
@@ -307,86 +284,97 @@
 
     def middle_later(c):
         value, _, _, mixed, sig = mixing(c)
-        hidden_v[c] = (mixed * sig * value).astype(BF16)
+        hidden_out[:, columns(c)] = (mixed * sig * value).astype(BF16)
 
     def middle_earlier(c):
         value, taps, shifted, mixed, sig = mixing(c)
         cot = cot_v[c].astype(F32)
-        grads[:, w:] = (cot * (mixed * sig)).astype(BF16)
+        grads[c, :, w:] = (cot * (mixed * sig)).astype(BF16)
         mixed_grad = cot * value * sig * (1.0 + mixed * (1.0 - sig))
         total = taps[count - 1] * mixed_grad
         for k in range(count - 1):
             total += taps[k] * up(mixed_grad, count - 1 - k)
-        grads[:, :w] = total.astype(BF16)
+        grads[c, :, :w] = total.astype(BF16)
         for k in range(count):
             small_v[c, k : k + 1, :] = jnp.sum(mixed_grad * shifted[k], axis=0, keepdims=True)
         small_v[c, count : count + 1, :] = jnp.sum(mixed_grad, axis=0, keepdims=True)
 
+    def rows_part(c, cols):
+        value = contract_last(grads[c - group + 1], weights[c - group + 1, cols, :])
+        for k in range(1, group):
+            at = c - group + 1 + k
+            value += contract_last(grads[at], weights[at, cols, :])
+        return value
+
     def add_rows(c):
-        def body(index, carry):
-            cols = pl.ds(pl.multiple_of(index * wide, wide), wide)
-            value = contract_last(grads[...], weights[c, cols, :])
-            acc[:, cols] += value
+        def body(p, carry):
+            cols = pl.ds(pl.multiple_of(p * cut, cut), cut)
+            acc[:, cols] += rows_part(c, cols)
             return carry
 
-        lax.fori_loop(0, model // wide, body, 0)
+        lax.fori_loop(0, q, body, 0)
 
     def last_rows(c):
-        def body(index, carry):
-            cols = pl.ds(pl.multiple_of(index * wide, wide), wide)
-            value = contract_last(grads[...], weights[c, cols, :])
-            rows_s[:, cols] = (acc[:, cols] + value).astype(BF16)
-            return carry
-
-        lax.fori_loop(0, model // wide, body, 0)
-        for p in range(q):
+        def body(p, carry):
+            cols = pl.ds(pl.multiple_of(p * cut, cut), cut)
+            rows_s[:, cols] = (acc[:, cols] + rows_part(c, cols)).astype(BF16)
             for k in range(1, side):
                 for half in range(2):
                     first_copy(half, k, p).start()
-
-    def make_terms(c):
+            return carry
+
+        lax.fori_loop(0, q, body, 0)
+
+    def make_terms(c, carry):
+        slot = lax.rem(c, 2)
+
         @pl.when(c >= 2)
         def _():
             term_copy(c - 2).wait_send()
 
-        def fill(target, which):
-            def body(d, carry):
-                rows = pl.ds(pl.multiple_of((2 * d + which) * depth, depth), depth)
-                value = jnp.dot(earlier_t[rows, :], grads[...], preferred_element_type=F32)
-                target[d] = value.astype(BF16)
-                return carry
-
-            lax.fori_loop(0, chips, body, 0)
-
-        fill(out_t.at[lax.rem(c, 2)], 1 - core)
+        half_rows = chips * depth
+        value = jnp.dot(earlier_t[...], grads[c], preferred_element_type=F32)
+        out_t[slot] = value[:half_rows].astype(BF16)
+        own_t[c] = value[half_rows:].astype(BF16)
         term_copy(c).start()
-        fill(own_t.at[c], core)
+        return carry
+
+    def wait_terms(c, carry):
+        term_copy(c).wait_recv()
+        return carry
 
     def transpose_rows():
         acc[...] = jnp.zeros_like(acc)
         small_v[...] = jnp.zeros_like(small_v)
-        step = math.gcd(model, 256)
-
-        def body(index, carry):
-            cols = pl.ds(pl.multiple_of(index * step, step), step)
-            earlier_t[cols, :] = earlier_v[:, cols].T
+
+        def body(d, carry):
+            cols = pl.ds(pl.multiple_of(d * 2 * depth, 2 * depth), 2 * depth)
+            value = earlier_v[:, cols].T
+            for which in range(2):
+                owner = jnp.where(core == which, chips + d, d)
+                rows = pl.ds(pl.multiple_of(owner * depth, depth), depth)
+                earlier_t[rows, :] = value[which * depth : (which + 1) * depth]
             return carry
 
-        lax.fori_loop(0, model // step, body, 0)
-
-    def compute(c):
+        lax.fori_loop(0, chips, body, 0)
+
+    def compute_first(c):
         @pl.when(c == 0)
         def _():
             load_rows(1).wait()
+            load_sum(0).wait()
+            load_sum(1).wait()
             transpose_rows()
 
         for o in range(chips):
             pair_copy(o, 1 - core, c).wait_recv()
         forward(earlier_v, c)
+
+    def compute_second(c):
         load_cot(c).wait()
         middle_earlier(c)
 
-        @pl.when(c < n - 1)
+        @pl.when(jnp.logical_and(c < n - 1, lax.rem(c, group) == group - 1))
         def _():
             add_rows(c)
 
@@ -396,16 +384,13 @@
             for k in range(1, fs_size):
                 small_copy(k, fs).start()
 
-        make_terms(c)
-
+    def compute_later(c):
         @pl.when(c == 0)
         def _():
             load_rows(0).wait()
 
         forward(later_v, c)
         middle_later(c)
-        store_hidden(c).start()
-        term_copy(c).wait_recv()
 
     def arrive(way, o, c, goes_on):
         line_copy(way, o, c).wait_recv()
@@ -416,18 +401,21 @@
 
         pair_copy(o, core, c).start()
 
+    def terms_of(c, d):
+        rows = pl.ds(pl.multiple_of(d * depth, depth), depth)
+        return own_t[c, rows, :].astype(F32) + pair_t[c, rows, :].astype(F32)
+
     def push(way, c, d, first_on_line):
         slot = ring_slot(way, c, d)
 
         @pl.when(first_on_line)
         def _():
-            slot[...] = (own_t[c, d].astype(F32) + pair_t[c, d].astype(F32)).astype(BF16)
+            slot[...] = terms_of(c, d).astype(BF16)
 
         @pl.when(jnp.logical_not(first_on_line))
         def _():
             ring_copy(way, c, d).wait_recv()
-            total = own_t[c, d].astype(F32) + pair_t[c, d].astype(F32) + slot[...].astype(F32)
-            slot[...] = total.astype(BF16)
+            slot[...] = (terms_of(c, d) + slot[...].astype(F32)).astype(BF16)
 
         ring_copy(way, c, d).start()
 
@@ -450,30 +438,43 @@
         return carry
 
     def finish_sum(c, carry):
-        load_sum(c, 0).wait()
-        load_sum(c, 1).wait()
-        base = own_t[c, z].astype(F32) + pair_t[c, z].astype(F32)
-        sums[c] += sizes.scale * base
-
-        @pl.when(z > 0)
+        def add(value):
+            gate_out[:, columns(c)] += sizes.scale * value[:, :w]
+            up_out[:, columns(c)] += sizes.scale * value[:, w:]
+
+        base = terms_of(c, z)
+
+        @pl.when(z == 0)
+        def _():
+            ring_copy(1, c, z).wait_recv()
+            add(base + ring_slot(1, c, z)[...].astype(F32))
+
+        @pl.when(z == last)
         def _():
             ring_copy(0, c, z).wait_recv()
-            sums[c] += sizes.scale * ring_slot(0, c, z)[...].astype(F32)
-
-        @pl.when(z < last)
-        def _():
+            add(base + ring_slot(0, c, z)[...].astype(F32))
+
+        @pl.when(jnp.logical_and(z > 0, z < last))
+        def _():
+            ring_copy(0, c, z).wait_recv()
             ring_copy(1, c, z).wait_recv()
-            sums[c] += sizes.scale * ring_slot(1, c, z)[...].astype(F32)
-
-        store_sum(c, 0).start()
-        store_sum(c, 1).start()
+            add(
+                base
+                + ring_slot(0, c, z)[...].astype(F32)
+                + ring_slot(1, c, z)[...].astype(F32)
+            )
+
         return carry
 
     far = jnp.maximum(z, last - z)
-    lag = max(n // 2, 1)
+
+    def termed(i):
+        return jnp.where(i >= n, n, jnp.clip(i, 0, max(n - 2, 0)))
 
     def pushed(i, hops):
-        return jnp.clip(i + 1 - lag * hops + jnp.maximum(i - (n - 1), 0), 0, n)
+        turn = i - (n - 1) - 2 * (hops - 1)
+        after = jnp.where(turn >= 1, jnp.clip(3 + (turn - 1) // 2, 0, n), 0)
+        return jnp.where(hops == 0, termed(i), after)
 
     def exchange(j):
         for half in range(2):
@@ -481,7 +482,7 @@
             @pl.when(jnp.logical_and(j >= 1, j <= q))
             def _():
                 p = j - 1
-                total = rows_s[piece(half, firsts[half], p), :].astype(F32)
+                total = rows_s[piece(half, firsts[half], p)].astype(F32)
                 for k in range(1, side):
                     first_copy(half, k, p).wait_recv()
                     total += first_in[half, k - 1, p].astype(F32)
@@ -498,10 +499,9 @@
                 total = second_in[half, 0, p].astype(F32)
                 for position in range(1, side):
                     total += second_in[half, position, p].astype(F32)
-                rows_buf[piece(half, firsts[half], p), :] = total.astype(BF16)
+                rows_out[piece(half, firsts[half], p)] = total.astype(BF16)
                 for k in range(1, side):
                     third_copy(half, k, p, firsts[half]).start()
-                store_rows(half, firsts[half], p).start()
 
             @pl.when(jnp.logical_and(j > 2 * q, j <= 3 * q))
             def _():
@@ -509,25 +509,34 @@
                 for k in range(1, side):
                     source = lax.rem(firsts[half] + side - k, side)
                     third_copy(half, k, p, source).wait_recv()
-                    store_rows(half, source, p).start()
+
+    at_end = jnp.logical_or(z == 0, z == last)
+
+    def send_own(c, carry):
+        load_weight(c, 0).wait()
+        load_weight(c, 1).wait()
+
+        @pl.when(z < last)
+        def _():
+            line_copy(0, z, c).start()
+
+        @pl.when(z > 0)
+        def _():
+            line_copy(1, z, c).start()
+
+        pair_copy(z, core, c).start()
+        return carry
+
+    @pl.when(at_end)
+    def _():
+        lax.fori_loop(0, n, send_own, 0)
 
     def step(s, carry):
         i = s - far
 
-        @pl.when(s < n)
-        def _():
-            load_weight(s, 0).wait()
-            load_weight(s, 1).wait()
-
-            @pl.when(z < last)
-            def _():
-                line_copy(0, z, s).start()
-
-            @pl.when(z > 0)
-            def _():
-                line_copy(1, z, s).start()
-
-            pair_copy(z, core, s).start()
+        @pl.when(jnp.logical_and(s < n, jnp.logical_not(at_end)))
+        def _():
+            send_own(s, 0)
 
         for k in range(1, chips):
             c = s - k
@@ -541,17 +550,31 @@
             def _():
                 arrive(1, z + k, c, z > 0)
 
+        lax.fori_loop(termed(i - 1), termed(i), make_terms, 0)
+
         @pl.when(jnp.logical_and(i >= 0, i < n))
         def _():
-            compute(i)
-
+            compute_first(i)
+
+        exchange(i - (n - 1))
+        lax.fori_loop(termed(i - 1), termed(i), wait_terms, 0)
         lax.fori_loop(pushed(i - 1, z), pushed(i, z), push_up, 0)
         lax.fori_loop(pushed(i - 1, last - z), pushed(i, last - z), push_down, 0)
-        lax.fori_loop(pushed(i - 1, far), pushed(i, far), finish_sum, 0)
-        exchange(i - (n - 1))
+        hops = jnp.where(at_end, 1, far)
+        lax.fori_loop(pushed(i - 1, hops), pushed(i, hops), finish_sum, 0)
+
+        @pl.when(jnp.logical_and(i >= 0, i < n))
+        def _():
+            compute_second(i)
+
+        @pl.when(jnp.logical_and(i >= n, i < 2 * n))
+        def _():
+            compute_later(i - n)
+
         return carry
 
-    end = max(n - 1 + 3 * q, n - 1 + -(-lag * last // 2))
+    turns = 2 * max(n - 3, 0) + 1 + 2 * max(last - 2, 0)
+    end = n - 1 + max(3 * q, n, turns)
     lax.fori_loop(0, end + last + 1, step, 0)
 
     small_buf[fs] = small_v[...]
@@ -597,9 +620,6 @@
         def _():
             term_copy(c).wait_send()
 
-        store_hidden(c).wait()
-        store_sum(c, 0).wait()
-        store_sum(c, 1).wait()
         return carry
 
     lax.fori_loop(0, n, drain, 0)
@@ -609,8 +629,18 @@
                 first_copy(half, k, p).wait_send()
                 second_copy(half, k, p, seconds[half]).wait_send()
                 third_copy(half, k, p, firsts[half]).wait_send()
-            for i in range(side):
-                store_rows(half, i, p).wait()
+
+
+def store_kernel(*refs):
+    count = len(refs) // 2
+    sources, targets, sems = refs[:count], refs[count : 2 * count], refs[-1]
+    copies = [
+        pltpu.make_async_copy(sources[at], targets[at], sems.at[at]) for at in range(count)
+    ]
+    for copy in copies:
+        copy.start()
+    for copy in copies:
+        copy.wait()
 
 
 def on_device(
@@ -632,7 +662,7 @@
     sizes = Sizes(
         lax.axis_size("fs"), lax.axis_size("tp"), tokens, model, depth, width, taps
     )
-    n, w, q, r = sizes.n, sizes.w, sizes.q, sizes.r
+    n, w, q, r, cut = sizes.n, sizes.w, sizes.q, sizes.r, sizes.cut
     chips, side, fs_size = sizes.chips, sizes.side, sizes.fs_size
     dma = pltpu.SemaphoreType.DMA
     whole = pl.BlockSpec(memory_space=pltpu.VMEM)
@@ -641,15 +671,15 @@
     outs = pl.pallas_call(
         functools.partial(kernel, sizes),
         out_shape=(
-            jax.ShapeDtypeStruct((tokens, width), BF16),
-            jax.ShapeDtypeStruct((tokens, model), BF16),
-            jax.ShapeDtypeStruct((depth, width), F32),
-            jax.ShapeDtypeStruct((depth, width), F32),
-            jax.ShapeDtypeStruct((taps, width), F32),
-            jax.ShapeDtypeStruct((1, width), F32),
+            pltpu.VMEM((tokens, width), BF16),
+            pltpu.VMEM((tokens, model), BF16),
+            pltpu.VMEM((depth, width), F32),
+            pltpu.VMEM((depth, width), F32),
+            pltpu.VMEM((taps, width), F32),
+            pltpu.VMEM((1, width), F32),
         ),
         in_specs=[far] * 7 + [whole] * 4,
-        out_specs=(far, far, far, far, whole, whole),
+        out_specs=(whole,) * 6,
         scratch_shapes=[
             pltpu.VMEM((tokens, model), BF16),
             pltpu.VMEM((tokens, model), BF16),
@@ -657,27 +687,21 @@
             pltpu.VMEM((n, tokens, w), BF16),
             pltpu.VMEM((n, model, 2 * w), BF16),
             pltpu.VMEM((tokens, 2 * w), BF16),
-            pltpu.VMEM((tokens, 2 * w), BF16),
-            pltpu.VMEM((n, tokens, w), BF16),
+            pltpu.VMEM((n, tokens, 2 * w), BF16),
             pltpu.VMEM((tokens, model), F32),
-            pltpu.VMEM((n, chips, depth, 2 * w), BF16),
-            pltpu.VMEM((2, chips, depth, 2 * w), BF16),
-            pltpu.VMEM((n, chips, depth, 2 * w), BF16),
+            pltpu.VMEM((n, chips * depth, 2 * w), BF16),
+            pltpu.VMEM((2, chips * depth, 2 * w), BF16),
+            pltpu.VMEM((n, chips * depth, 2 * w), BF16),
             pltpu.VMEM((2, n, max(chips - 1, 1), depth, 2 * w), BF16),
-            pltpu.VMEM((n, depth, 2 * w), F32),
             pltpu.VMEM((tokens, model), BF16),
-            pltpu.VMEM((2, links, q, r, model), BF16),
-            pltpu.VMEM((2, side, q, r, model), BF16),
-            pltpu.VMEM((tokens, model), BF16),
+            pltpu.VMEM((2, links, q, r, cut), BF16),
+            pltpu.VMEM((2, side, q, r, cut), BF16),
             pltpu.VMEM((n, 8 * -(-(taps + 1) // 8), w), F32),
             pltpu.VMEM((fs_size, n, 8 * -(-(taps + 1) // 8), w), F32),
             dma((n, 2)),
             dma((2,)),
             dma((n,)),
-            dma((n, 2)),
-            dma((n, 2)),
-            dma((n,)),
-            dma((2, side, q)),
+            dma((2,)),
             dma((2, n, chips)),
             dma((n, chips)),
             dma((n, chips)),
@@ -705,15 +729,15 @@
         taps_grad_sum,
         bias_grad_sum[None],
     )
-    hidden_later, input_grad, gate_grad_out, up_grad_out, taps_grad_out, bias_grad_out = outs
-    return (
-        hidden_later,
-        input_grad,
-        gate_grad_out,
-        up_grad_out,
-        taps_grad_out,
-        bias_grad_out[0],
-    )
+    stored = pl.pallas_call(
+        store_kernel,
+        out_shape=tuple(jax.ShapeDtypeStruct(out.shape, out.dtype) for out in outs),
+        in_specs=[whole] * len(outs),
+        out_specs=(far,) * len(outs),
+        scratch_shapes=[dma((len(outs),))],
+        compiler_params=pltpu.CompilerParams(vmem_limit_bytes=1024 * 1024),
+    )(*[pltpu.with_memory_space_constraint(out, pltpu.VMEM) for out in outs])
+    return stored[:5] + (stored[5][0],)
 
 
 def solution(mesh):

time: 166 us -> 142 us (0.86)
  Pallas kernels: 158 us -> 142 us
  local copies, waits for them, and re-layouts: 7.93 us -> 0 us
    pallas_call x1 -> x2, Pallas kernels: 158 us -> 142 us  [the longest x1 139 us: on_device(): pl.pallas_call(functools.partial(kernel, sizes), out_shape=(pltpu.VMEM((t...]
    unnamed x16 -> x0, local copies, waits for them, and re-layouts: 7.93 us -> none
where the time goes in v2:
time: 142 us
  Pallas kernels  142 us (100%)
    pallas_call x1, Pallas kernels, on_device(): pl.pallas_call(functools.partial(kernel, sizes), out_shape=(pltpu.VMEM((t...  139 us
    pallas_call x1, Pallas kernels, on_device(): pl.pallas_call(store_kernel, out_shape=tuple((jax.ShapeDtypeStruct(out.sh...  2.9 us

profile of v2, /device:TPU:0, one launch (start us, length us, event | category | flops | bytes accessed | tf_op | source)
XLA Modules:
  0.0 142.2 jit_solution(3315316329728414992)
XLA Ops:
  0.6 138.6 %shard_map.154 = (bf16[768,1024]{1,0:T(8,128)(2,1)S(1)}, bf16[768,2048]{1,0:T(8,128)(2,1)S(1)}, f32[256,1024]{1,0:T(8,128)S(1)}, f32[256,1024]{1,0:T(8,128)S(1)}...) custom-call(bf16[768,2048]{1,0:T(8,128)(2,1)} %later_hbm.1, bf16[768,2048]{1,0:T(8,128)(2,1)} %earlier_hbm.1, ...), custom_call_target="tpu_custom_call" | custom-call | tf_op jit(solution)/shard_map/pallas_call | solution.py:671
  139.3 2.9 %shard_map.155 = (bf16[768,1024]{1,0:T(8,128)(2,1)}, bf16[768,2048]{1,0:T(8,128)(2,1)}, f32[256,1024]{1,0:T(8,128)}, f32[256,1024]{1,0:T(8,128)}, f32[3,1024]{1,0:T(4,128)}, /*index=5*/f32[1,1024]{1,0:T(1,128)}) custom-call(bf16[768,1024]{1,0:T(8,128)(2,1)S(1)} %get-tuple-element.18.refs_0_, bf16[768,2048]{1,0:T(8,128)(2,1)S(1)} %get-tuple-element.19.refs_1_, ...), custom_call_target="tpu_custom_call" | custom-call | tf_op jit(solution)/shard_map/pallas_call | solution.py:732

commit v3 on v2

--- a/solution.py
+++ b/solution.py
@@ -9,7 +9,7 @@
 from jax.sharding import PartitionSpec as P
 
 MESH = pl.DeviceIdType.MESH
-VMEM_BYTES = 56 * 1024 * 1024
+VMEM_BYTES = 57 * 1024 * 1024
 FORWARD_ROWS = 768
 F32, BF16 = jnp.float32, jnp.bfloat16
 
@@ -45,8 +45,9 @@
         self.n = width // self.w
         self.taps = taps
         self.group = math.gcd(self.n, 2)
+        self.tail = min(self.n, 2 * self.group)
         self.r = tokens // (2 * self.side)
-        self.q = max(q for q in (1, 2, 4) if model % (128 * q) == 0)
+        self.q = max(q for q in (1, 2, 4, 8) if model % (128 * q) == 0)
         self.cut = model // self.q
         self.scale = 1.0 / math.sqrt(tokens * fs_size)
 
@@ -60,10 +61,10 @@
     up_hbm,
     gate_sum_hbm,
     up_sum_hbm,
-    taps_ref,
-    bias_ref,
-    taps_sum_ref,
-    bias_sum_ref,
+    taps_hbm,
+    bias_hbm,
+    taps_sum_hbm,
+    bias_sum_hbm,
     hidden_out,
     rows_out,
     gate_out,
@@ -83,10 +84,22 @@
     pair_t,
     ring,
     rows_s,
+    help_in,
+    help_out,
+    help_send,
+    help_recv,
+    back_send,
+    back_recv,
     first_in,
     second_in,
     small_v,
+    small_in,
     small_buf,
+    taps_ref,
+    bias_ref,
+    taps_sum_ref,
+    bias_sum_ref,
+    mix_load,
     weight_load,
     rows_load,
     cot_load,
@@ -109,7 +122,7 @@
     small_recv,
 ):
     n, w, q, r, cut = sizes.n, sizes.w, sizes.q, sizes.r, sizes.cut
-    group = sizes.group
+    group, tail = sizes.group, sizes.tail
     chips, side, depth = sizes.chips, sizes.side, sizes.depth
     fs_size, tokens, model = sizes.fs_size, sizes.tokens, sizes.model
     count = sizes.taps
@@ -119,6 +132,9 @@
     z = fs // 2
     core = lax.rem(fs, 2)
     partner = 2 * z + 1 - core
+    at_end = jnp.logical_or(z == 0, z == last)
+    helped = chips >= 4
+    helper = jnp.logical_and(helped, jnp.logical_or(z == 1, z == last - 1))
     neighbours = (lax.rem(fs + 2, fs_size), lax.rem(fs + fs_size - 2, fs_size))
     ty = tp // side
     tx = lax.rem(tp, side)
@@ -155,14 +171,21 @@
     def load_cot(c):
         return pltpu.make_async_copy(cot_hbm.at[:, columns(c)], cot_v.at[c], cot_load.at[c])
 
+    def load_mix(which):
+        sources = (taps_hbm, bias_hbm, taps_sum_hbm, bias_sum_hbm)
+        targets = (taps_ref, bias_ref, taps_sum_ref, bias_sum_ref)
+        return pltpu.make_async_copy(sources[which], targets[which], mix_load.at[which])
+
     def load_sum(which):
         return pltpu.make_async_copy(
             (gate_sum_hbm, up_sum_hbm)[which], (gate_out, up_out)[which], sum_load.at[which]
         )
 
+    def block_of(half, i):
+        return pl.ds(pl.multiple_of((half * side + i) * r, r), r)
+
     def piece(half, i, p):
-        rows = pl.ds(pl.multiple_of((half * side + i) * r, r), r)
-        return rows, pl.ds(pl.multiple_of(p * cut, cut), cut)
+        return block_of(half, i), pl.ds(pl.multiple_of(p * cut, cut), cut)
 
     def remote(source, target, send, recv, device):
         return pltpu.make_async_remote_copy(
@@ -204,11 +227,21 @@
         slot = ring.at[at]
         return remote(slot, slot, ring_send.at[at], ring_recv.at[at], {"fs": neighbours[way]})
 
+    def source_of(half, i, p):
+        if isinstance(p, int) and p == q:
+            return help_in.at[block_of(half, i)]
+        return rows_s.at[piece(half, i, p)]
+
+    def target_of(half, i, p):
+        if isinstance(p, int) and p == q:
+            return help_out.at[block_of(half, i)]
+        return rows_out.at[piece(half, i, p)]
+
     def first_copy(half, k, p):
         peer, device = first_peer(half, k)
         at = (half, k - 1, p)
         return remote(
-            rows_s.at[piece(half, peer, p)],
+            source_of(half, peer, p),
             first_in.at[at],
             first_send.at[at],
             first_recv.at[at],
@@ -223,28 +256,83 @@
 
     def third_copy(half, k, p, shown):
         _, device = first_peer(half, k)
-        block = rows_out.at[piece(half, shown, p)]
+        ref = target_of(half, shown, p)
         at = (half, k - 1, p)
-        return remote(block, block, third_send.at[at], third_recv.at[at], {"tp": device})
-
-    def small_copy(k, slot):
+        return remote(ref, ref, third_send.at[at], third_recv.at[at], {"tp": device})
+
+    def help_copy():
+        device = jnp.where(z == 0, neighbours[0], neighbours[1])
+        source = rows_s.at[:, pl.ds(0, cut)]
+        return remote(source, help_in, help_send.at[0], help_recv.at[0], {"fs": device})
+
+    def back_copy(half, i):
+        device = jnp.where(z == 1, neighbours[1], neighbours[0])
+        at = (half, i)
         return remote(
-            small_v,
-            small_buf.at[slot],
-            small_send.at[k - 1],
-            small_recv.at[k - 1],
-            {"fs": lax.rem(fs + k, fs_size)},
+            help_out.at[block_of(half, i)],
+            rows_out.at[piece(half, i, 0)],
+            back_send.at[at],
+            back_recv.at[at],
+            {"fs": device},
         )
+
+    def small_pair():
+        return remote(small_v, small_in, small_send.at[2, 0], small_recv.at[z], {"fs": partner})
+
+    def small_copy(way, o):
+        ref = small_buf.at[o]
+        return remote(
+            ref, ref, small_send.at[way, o], small_recv.at[o], {"fs": neighbours[way]}
+        )
+
+    def send_small():
+        small_pair().wait_recv()
+        low = jnp.where(core == 0, small_v[...], small_in[...])
+        high = jnp.where(core == 0, small_in[...], small_v[...])
+        small_buf[z] = low + high
+
+        @pl.when(z < last)
+        def _():
+            small_copy(0, z).start()
+
+        @pl.when(z > 0)
+        def _():
+            small_copy(1, z).start()
+
+    def pass_small(k):
+        @pl.when(z - k >= 0)
+        def _():
+            small_copy(0, z - k).wait_recv()
+
+            @pl.when(z < last)
+            def _():
+                small_copy(0, z - k).start()
+
+        @pl.when(z + k <= last)
+        def _():
+            small_copy(1, z + k).wait_recv()
+
+            @pl.when(z > 0)
+            def _():
+                small_copy(1, z + k).start()
 
     for c in range(n):
         load_weight(c, 0).start()
         load_weight(c, 1).start()
 
     barrier = pltpu.get_barrier_semaphore()
-    for k in range(1, fs_size):
-        pl.semaphore_signal(
-            barrier, inc=1, device_id={"fs": lax.rem(fs + k, fs_size)}, device_id_type=MESH
-        )
+    def greet(device):
+        pl.semaphore_signal(barrier, inc=1, device_id={"fs": device}, device_id_type=MESH)
+
+    @pl.when(z < last)
+    def _():
+        greet(neighbours[0])
+
+    @pl.when(z > 0)
+    def _():
+        greet(neighbours[1])
+
+    greet(partner)
     for half in range(2):
         for k in range(1, side):
             pl.semaphore_signal(
@@ -255,10 +343,13 @@
     for c in range(n):
         load_cot(c).start()
     load_rows(0).start()
+    for which in range(4):
+        load_mix(which).start()
     load_sum(0).start()
     load_sum(1).start()
 
-    pl.semaphore_wait(barrier, fs_size - 1 + 2 * (side - 1))
+    expected = 1 + 2 * (side - 1) + jnp.where(z < last, 1, 0) + jnp.where(z > 0, 1, 0)
+    pl.semaphore_wait(barrier, expected)
 
     block = math.gcd(tokens, FORWARD_ROWS)
 
@@ -299,28 +390,42 @@
             small_v[c, k : k + 1, :] = jnp.sum(mixed_grad * shifted[k], axis=0, keepdims=True)
         small_v[c, count : count + 1, :] = jnp.sum(mixed_grad, axis=0, keepdims=True)
 
-    def rows_part(c, cols):
-        value = contract_last(grads[c - group + 1], weights[c - group + 1, cols, :])
-        for k in range(1, group):
-            at = c - group + 1 + k
+    def rows_part(c, chunks, cols):
+        value = contract_last(grads[c - chunks + 1], weights[c - chunks + 1, cols, :])
+        for k in range(1, chunks):
+            at = c - chunks + 1 + k
             value += contract_last(grads[at], weights[at, cols, :])
         return value
 
     def add_rows(c):
+        wide = math.gcd(model, 512)
+
         def body(p, carry):
-            cols = pl.ds(pl.multiple_of(p * cut, cut), cut)
-            acc[:, cols] += rows_part(c, cols)
+            cols = pl.ds(pl.multiple_of(p * wide, wide), wide)
+            acc[:, cols] += rows_part(c, group, cols)
             return carry
 
-        lax.fori_loop(0, q, body, 0)
+        lax.fori_loop(0, model // wide, body, 0)
+
+    def kept(p):
+        return jnp.logical_not(jnp.logical_and(helped, jnp.logical_and(at_end, p == 0)))
+
+    def start_first(p):
+        @pl.when(kept(p))
+        def _():
+            for k in range(1, side):
+                for half in range(2):
+                    first_copy(half, k, p).start()
+
+        @pl.when(jnp.logical_not(kept(p)))
+        def _():
+            help_copy().start()
 
     def last_rows(c):
         def body(p, carry):
             cols = pl.ds(pl.multiple_of(p * cut, cut), cut)
-            rows_s[:, cols] = (acc[:, cols] + rows_part(c, cols)).astype(BF16)
-            for k in range(1, side):
-                for half in range(2):
-                    first_copy(half, k, p).start()
+            rows_s[:, cols] = (acc[:, cols] + rows_part(c, tail, cols)).astype(BF16)
+            start_first(p)
             return carry
 
         lax.fori_loop(0, q, body, 0)
@@ -362,6 +467,8 @@
         @pl.when(c == 0)
         def _():
             load_rows(1).wait()
+            for which in range(4):
+                load_mix(which).wait()
             load_sum(0).wait()
             load_sum(1).wait()
             transpose_rows()
@@ -374,15 +481,14 @@
         load_cot(c).wait()
         middle_earlier(c)
 
-        @pl.when(jnp.logical_and(c < n - 1, lax.rem(c, group) == group - 1))
+        @pl.when(jnp.logical_and(c < n - tail, lax.rem(c, group) == group - 1))
         def _():
             add_rows(c)
 
         @pl.when(c == n - 1)
         def _():
             last_rows(c)
-            for k in range(1, fs_size):
-                small_copy(k, fs).start()
+            small_pair().start()
 
     def compute_later(c):
         @pl.when(c == 0)
@@ -472,45 +578,167 @@
         return jnp.where(i >= n, n, jnp.clip(i, 0, max(n - 2, 0)))
 
     def pushed(i, hops):
-        turn = i - (n - 1) - 2 * (hops - 1)
-        after = jnp.where(turn >= 1, jnp.clip(3 + (turn - 1) // 2, 0, n), 0)
+        turn = i - (n - 1)
+        near = jnp.clip(jnp.maximum(3 + (turn - 1) // 2, turn - 2), 0, n)
+        near = jnp.where(turn >= 1, near, 0)
+        after = jnp.where(hops == 1, near, jnp.clip(turn + 1 - 2 * hops, 0, n))
         return jnp.where(hops == 0, termed(i), after)
 
+    batch = math.gcd(q, 2)
+    rounds = q // batch
+
+    hold = jnp.where(helper, rounds - 1, 0)
+    turns = max(n + 4, n + 2 * (last - 1), 6 + 2 * last, 3 * rounds, 2 * rounds + 3)
+    end = n - 1 + turns
+
     def exchange(j):
-        for half in range(2):
-
-            @pl.when(jnp.logical_and(j >= 1, j <= q))
+        def during(first, action):
+            @pl.when(jnp.logical_and(j > first, j <= first + rounds))
             def _():
-                p = j - 1
-                total = rows_s[piece(half, firsts[half], p)].astype(F32)
+                for at in range(batch):
+                    p = (j - 1 - first) * batch + at
+
+                    @pl.when(kept(p))
+                    def _():
+                        for half in range(2):
+                            action(half, p)
+
+        during(0, exchange_first)
+        during(rounds, exchange_second)
+        if helped:
+            assist(j - 2 * rounds)
+        during(rounds + hold, exchange_send)
+
+    def assist(turn):
+        @pl.when(jnp.logical_and(helper, turn == 0))
+        def _():
+            help_copy().wait_recv()
+            for k in range(1, side):
+                for half in range(2):
+                    first_copy(half, k, q).start()
+
+        @pl.when(jnp.logical_and(helper, turn == 1))
+        def _():
+            for half in range(2):
+                exchange_first(half, q)
+
+        @pl.when(jnp.logical_and(helper, turn == 2))
+        def _():
+            for half in range(2):
+                exchange_second(half, q)
+                exchange_send(half, q)
+                back_copy(half, firsts[half]).start()
+
+        @pl.when(jnp.logical_and(helper, turn == 3))
+        def _():
+            for half in range(2):
                 for k in range(1, side):
-                    first_copy(half, k, p).wait_recv()
-                    total += first_in[half, k - 1, p].astype(F32)
-                second_in[half, seconds[half], p] = total.astype(BF16)
-                for k in range(1, side):
-                    second_copy(half, k, p, seconds[half]).start()
-
-            @pl.when(jnp.logical_and(j > q, j <= 2 * q))
+                    shown = lax.rem(firsts[half] + side - k, side)
+                    third_copy(half, k, q, shown).wait_recv()
+                    back_copy(half, shown).start()
+
+    def exchange_first(half, p):
+        total = source_of(half, firsts[half], p)[...].astype(F32)
+        for k in range(1, side):
+            first_copy(half, k, p).wait_recv()
+            total += first_in[half, k - 1, p].astype(F32)
+        second_in[half, seconds[half], p] = total.astype(BF16)
+        for k in range(1, side):
+            second_copy(half, k, p, seconds[half]).start()
+
+    def exchange_second(half, p):
+        for k in range(1, side):
+            position = lax.rem(seconds[half] + side - k, side)
+            second_copy(half, k, p, position).wait_recv()
+        total = second_in[half, 0, p].astype(F32)
+        for position in range(1, side):
+            total += second_in[half, position, p].astype(F32)
+        target_of(half, firsts[half], p)[...] = total.astype(BF16)
+
+    def exchange_send(half, p):
+        for k in range(1, side):
+            third_copy(half, k, p, firsts[half]).start()
+
+    def exchange_third(half, p):
+        for k in range(1, side):
+            third_copy(half, k, p, lax.rem(firsts[half] + side - k, side)).wait_recv()
+
+    def finish_small():
+        for c in range(n):
+            total = small_buf[0, c]
+            for source in range(1, chips):
+                total += small_buf[source, c]
+            total = sizes.scale * total
+            cols = slice(c * w, (c + 1) * w)
+            taps_out[:, cols] = taps_sum_ref[:, cols] + total[:count]
+            bias_out[:, cols] = bias_sum_ref[:, cols] + total[count : count + 1]
+        small_pair().wait_send()
+
+    def drain_gather(c, carry):
+        def over_chips(d, inner):
+            pair_copy(d, core, c).wait_send()
+
+            @pl.when(jnp.logical_and(d <= z, z < last))
             def _():
-                p = j - 1 - q
-                for k in range(1, side):
-                    position = lax.rem(seconds[half] + side - k, side)
-                    second_copy(half, k, p, position).wait_recv()
-                total = second_in[half, 0, p].astype(F32)
-                for position in range(1, side):
-                    total += second_in[half, position, p].astype(F32)
-                rows_out[piece(half, firsts[half], p)] = total.astype(BF16)
-                for k in range(1, side):
-                    third_copy(half, k, p, firsts[half]).start()
-
-            @pl.when(jnp.logical_and(j > 2 * q, j <= 3 * q))
+                line_copy(0, d, c).wait_send()
+
+            @pl.when(jnp.logical_and(d >= z, z > 0))
             def _():
-                p = j - 1 - 2 * q
-                for k in range(1, side):
-                    source = lax.rem(firsts[half] + side - k, side)
-                    third_copy(half, k, p, source).wait_recv()
-
-    at_end = jnp.logical_or(z == 0, z == last)
+                line_copy(1, d, c).wait_send()
+
+            return inner
+
+        return lax.fori_loop(0, chips, over_chips, carry)
+
+    def drain_ring(c, carry):
+        for d in range(chips):
+            if d > 0:
+
+                @pl.when(d > z)
+                def _():
+                    ring_copy(0, c, d).wait_send()
+
+            if d < last:
+
+                @pl.when(d < z)
+                def _():
+                    ring_copy(1, c, d).wait_send()
+
+        return carry
+
+    def drain_first():
+        for p in range(q):
+
+            @pl.when(kept(p))
+            def _():
+                for half in range(2):
+                    for k in range(1, side):
+                        first_copy(half, k, p).wait_send()
+
+    def drain_second():
+        for p in range(q):
+
+            @pl.when(kept(p))
+            def _():
+                for half in range(2):
+                    for k in range(1, side):
+                        second_copy(half, k, p, seconds[half]).wait_send()
+
+    def drain_early(j):
+        @pl.when(j == rounds)
+        def _():
+            lax.fori_loop(0, n, drain_gather, 0)
+            for c in range(max(n - 2, 0), n):
+                term_copy(c).wait_send()
+
+        @pl.when(j == 2 * rounds + 1)
+        def _():
+            drain_first()
+
+    def drain_late():
+        lax.fori_loop(0, n - 1, drain_ring, 0)
+        drain_second()
+        finish_small()
 
     def send_own(c, carry):
         load_weight(c, 0).wait()
@@ -556,12 +784,29 @@
         def _():
             compute_first(i)
 
+        drain_early(i - (n - 1))
         exchange(i - (n - 1))
         lax.fori_loop(termed(i - 1), termed(i), wait_terms, 0)
+        @pl.when(i == n)
+        def _():
+            send_small()
+
+        turn = i - (n + 4)
+        inside = jnp.logical_and(turn >= 2, turn <= 2 * last)
+
+        @pl.when(jnp.logical_and(inside, lax.rem(turn, 2) == 0))
+        def _():
+            pass_small(turn // 2)
+
         lax.fori_loop(pushed(i - 1, z), pushed(i, z), push_up, 0)
         lax.fori_loop(pushed(i - 1, last - z), pushed(i, last - z), push_down, 0)
-        hops = jnp.where(at_end, 1, far)
-        lax.fori_loop(pushed(i - 1, hops), pushed(i, hops), finish_sum, 0)
+        finish = jnp.where(at_end, i - 1, i)
+        hops = jnp.where(at_end, 2, far)
+        lax.fori_loop(pushed(finish - 1, hops), pushed(finish, hops), finish_sum, 0)
+
+        @pl.when(i == end)
+        def _():
+            drain_late()
 
         @pl.when(jnp.logical_and(i >= 0, i < n))
         def _():
@@ -573,62 +818,49 @@
 
         return carry
 
-    turns = 2 * max(n - 3, 0) + 1 + 2 * max(last - 2, 0)
-    end = n - 1 + max(3 * q, n, turns)
     lax.fori_loop(0, end + last + 1, step, 0)
 
-    small_buf[fs] = small_v[...]
-    for k in range(1, fs_size):
-        small_copy(k, lax.rem(fs + fs_size - k, fs_size)).wait_recv()
-    for c in range(n):
-        total = small_buf[0, c]
-        for source in range(1, fs_size):
-            total += small_buf[source, c]
-        total = sizes.scale * total
-        cols = slice(c * w, (c + 1) * w)
-        taps_out[:, cols] = taps_sum_ref[:, cols] + total[:count]
-        bias_out[:, cols] = bias_sum_ref[:, cols] + total[count : count + 1]
-
-    for k in range(1, fs_size):
-        small_copy(k, fs).wait_send()
-
-    def drain(c, carry):
-        def over_chips(d, inner):
-            pair_copy(d, core, c).wait_send()
-
-            @pl.when(jnp.logical_and(d <= z, z < last))
-            def _():
-                line_copy(0, d, c).wait_send()
-
-            @pl.when(jnp.logical_and(d >= z, z > 0))
-            def _():
-                line_copy(1, d, c).wait_send()
-
-            @pl.when(d > z)
-            def _():
-                ring_copy(0, c, d).wait_send()
-
-            @pl.when(d < z)
-            def _():
-                ring_copy(1, c, d).wait_send()
-
-            return inner
-
-        lax.fori_loop(0, chips, over_chips, 0)
-
-        @pl.when(c >= n - 2)
-        def _():
-            term_copy(c).wait_send()
+    lax.fori_loop(n - 1, n, drain_ring, 0)
+
+    def drain_small(o, carry):
+        @pl.when(jnp.logical_and(o <= z, z < last))
+        def _():
+            small_copy(0, o).wait_send()
+
+        @pl.when(jnp.logical_and(o >= z, z > 0))
+        def _():
+            small_copy(1, o).wait_send()
 
         return carry
 
-    lax.fori_loop(0, n, drain, 0)
-    for half in range(2):
-        for p in range(q):
-            for k in range(1, side):
-                first_copy(half, k, p).wait_send()
-                second_copy(half, k, p, seconds[half]).wait_send()
-                third_copy(half, k, p, firsts[half]).wait_send()
+    lax.fori_loop(0, chips, drain_small, 0)
+    for p in range(q):
+
+        @pl.when(kept(p))
+        def _():
+            for half in range(2):
+                exchange_third(half, p)
+                for k in range(1, side):
+                    third_copy(half, k, p, firsts[half]).wait_send()
+
+    if helped:
+
+        @pl.when(at_end)
+        def _():
+            help_copy().wait_send()
+            for half in range(2):
+                for i in range(side):
+                    back_copy(half, i).wait_recv()
+
+        @pl.when(helper)
+        def _():
+            for half in range(2):
+                for k in range(1, side):
+                    first_copy(half, k, q).wait_send()
+                    second_copy(half, k, q, seconds[half]).wait_send()
+                    third_copy(half, k, q, firsts[half]).wait_send()
+                for i in range(side):
+                    back_copy(half, i).wait_send()
 
 
 def store_kernel(*refs):
@@ -678,7 +910,7 @@
             pltpu.VMEM((taps, width), F32),
             pltpu.VMEM((1, width), F32),
         ),
-        in_specs=[far] * 7 + [whole] * 4,
+        in_specs=[far] * 11,
         out_specs=(whole,) * 6,
         scratch_shapes=[
             pltpu.VMEM((tokens, model), BF16),
@@ -694,10 +926,22 @@
             pltpu.VMEM((n, chips * depth, 2 * w), BF16),
             pltpu.VMEM((2, n, max(chips - 1, 1), depth, 2 * w), BF16),
             pltpu.VMEM((tokens, model), BF16),
-            pltpu.VMEM((2, links, q, r, cut), BF16),
-            pltpu.VMEM((2, side, q, r, cut), BF16),
+            pltpu.VMEM((tokens, cut), BF16),
+            pltpu.VMEM((tokens, cut), BF16),
+            dma((1,)),
+            dma((1,)),
+            dma((2, side)),
+            dma((2, side)),
+            pltpu.VMEM((2, links, q + 1, r, cut), BF16),
+            pltpu.VMEM((2, side, q + 1, r, cut), BF16),
             pltpu.VMEM((n, 8 * -(-(taps + 1) // 8), w), F32),
-            pltpu.VMEM((fs_size, n, 8 * -(-(taps + 1) // 8), w), F32),
+            pltpu.VMEM((n, 8 * -(-(taps + 1) // 8), w), F32),
+            pltpu.VMEM((chips, n, 8 * -(-(taps + 1) // 8), w), F32),
+            pltpu.VMEM((taps, width), F32),
+            pltpu.VMEM((1, width), F32),
+            pltpu.VMEM((taps, width), F32),
+            pltpu.VMEM((1, width), F32),
+            dma((4,)),
             dma((n, 2)),
             dma((2,)),
             dma((n,)),
@@ -711,8 +955,8 @@
             dma((2, n, max(chips - 1, 1))),
             dma((2, n, max(chips - 1, 1))),
         ]
-        + [dma((2, links, q))] * 6
-        + [dma((fs_size - 1,))] * 2,
+        + [dma((2, links, q + 1))] * 6
+        + [dma((3, chips)), dma((chips,))],
         compiler_params=pltpu.CompilerParams(
             collective_id=0, has_side_effects=True, vmem_limit_bytes=VMEM_BYTES
         ),

time: 142 us -> 133 us (0.937)
  Pallas kernels: 142 us -> 132 us
    pallas_call x1, Pallas kernels: 139 us -> 129 us  [on_device(): pl.pallas_call(functools.partial(kernel, sizes), out_shape=(pltpu.VMEM((t...]
where the time goes in v3:
time: 133 us
  Pallas kernels  132 us (99%)
    pallas_call x1, Pallas kernels, on_device(): pl.pallas_call(functools.partial(kernel, sizes), out_shape=(pltpu.VMEM((t...  129 us
    pallas_call x1, Pallas kernels, on_device(): pl.pallas_call(store_kernel, out_shape=tuple((jax.ShapeDtypeStruct(out.sh...  2.9 us

profile of v3, /device:TPU:0, one launch (start us, length us, event | category | flops | bytes accessed | tf_op | source)
XLA Modules:
  0.0 132.7 jit_solution(12665404861445718862)
XLA Ops:
  0.6 129.2 %shard_map.154 = (bf16[768,1024]{1,0:T(8,128)(2,1)S(1)}, bf16[768,2048]{1,0:T(8,128)(2,1)S(1)}, f32[256,1024]{1,0:T(8,128)S(1)}, f32[256,1024]{1,0:T(8,128)S(1)}...) custom-call(bf16[768,2048]{1,0:T(8,128)(2,1)} %later_hbm.1, bf16[768,2048]{1,0:T(8,128)(2,1)} %earlier_hbm.1, ...), custom_call_target="tpu_custom_call" | custom-call | tf_op jit(solution)/shard_map/pallas_call | solution.py:903
  129.8 2.9 %shard_map.155 = (bf16[768,1024]{1,0:T(8,128)(2,1)}, bf16[768,2048]{1,0:T(8,128)(2,1)}, f32[256,1024]{1,0:T(8,128)}, f32[256,1024]{1,0:T(8,128)}, f32[3,1024]{1,0:T(4,128)}, /*index=5*/f32[1,1024]{1,0:T(1,128)}) custom-call(bf16[768,1024]{1,0:T(8,128)(2,1)S(1)} %get-tuple-element.18.refs_0_, bf16[768,2048]{1,0:T(8,128)(2,1)S(1)} %get-tuple-element.19.refs_1_, ...), custom_call_target="tpu_custom_call" | custom-call | tf_op jit(solution)/shard_map/pallas_call | solution.py:976

commit v4 on v3

--- a/solution.py
+++ b/solution.py
@@ -111,7 +111,6 @@
     term_send,
     term_recv,
     ring_send,
-    ring_recv,
     first_send,
     first_recv,
     second_send,
@@ -160,16 +159,21 @@
         return pltpu.make_async_copy(
             source.at[:, columns(c)],
             weights.at[c, own_rows(core), pl.ds(which * w, w)],
-            weight_load.at[c, which],
-        )
+            weight_load.at[which],
+        )
+
+    def wait_weights():
+        for which in range(2):
+            ref = weights.at[:, own_rows(core), pl.ds(which * w, w)]
+            pltpu.make_async_copy(ref, ref, weight_load.at[which]).wait()
 
     def load_rows(which):
         return pltpu.make_async_copy(
             (later_hbm, earlier_hbm)[which], (later_v, earlier_v)[which], rows_load.at[which]
         )
 
-    def load_cot(c):
-        return pltpu.make_async_copy(cot_hbm.at[:, columns(c)], cot_v.at[c], cot_load.at[c])
+    def load_cot():
+        return pltpu.make_async_copy(cot_hbm, cot_v, cot_load.at[0])
 
     def load_mix(which):
         sources = (taps_hbm, bias_hbm, taps_sum_hbm, bias_sum_hbm)
@@ -203,18 +207,33 @@
     def line_copy(way, o, c):
         ref = shard(o, core, c)
         return remote(
-            ref, ref, line_send.at[way, c, o], line_recv.at[c, o], {"fs": neighbours[way]}
-        )
-
-    def pair_copy(o, which, c):
-        ref = shard(o, which, c)
-        return remote(ref, ref, pair_send.at[c, o], pair_recv.at[c, o], {"fs": partner})
+            ref, ref, line_send.at[way, o], line_recv.at[c, o], {"fs": neighbours[way]}
+        )
+
+    def line_sent(way, o):
+        rows = pl.ds(pl.multiple_of((2 * o + core) * depth, depth), depth)
+        ref = weights.at[:, rows]
+        return remote(
+            ref, ref, line_send.at[way, o], line_recv.at[0, 0], {"fs": neighbours[way]}
+        )
+
+    def pair_copy(o, c):
+        ref = shard(o, core, c)
+        return remote(ref, ref, pair_send.at[0], pair_recv.at[c], {"fs": partner})
+
+    def pair_received(c):
+        ref = weights.at[c, pl.ds(0, chips * depth)]
+        return remote(ref, ref, pair_send.at[0], pair_recv.at[c], {"fs": partner})
+
+    def pair_sent():
+        ref = weights.at[:, pl.ds(0, chips * depth)]
+        return remote(ref, ref, pair_send.at[0], pair_recv.at[0], {"fs": partner})
 
     def term_copy(c):
         return remote(
             out_t.at[lax.rem(c, 2)],
             pair_t.at[c],
-            term_send.at[c],
+            term_send.at[lax.rem(c, 2)],
             term_recv.at[c],
             {"fs": partner},
         )
@@ -222,10 +241,27 @@
     def ring_slot(way, c, d):
         return ring.at[way, c, d - 1 if way == 0 else d]
 
-    def ring_copy(way, c, d):
-        at = (way, c, d - 1 if way == 0 else d)
-        slot = ring.at[at]
-        return remote(slot, slot, ring_send.at[at], ring_recv.at[at], {"fs": neighbours[way]})
+    def ring_copy(way, c, d, at):
+        index = d - 1 if way == 0 else d
+        recv = line_recv.at[c, jnp.where(d == at, chips + way, d)]
+        slot = ring.at[way, c, index]
+        return remote(
+            slot,
+            slot,
+            ring_send.at[way, index],
+            recv,
+            {"fs": neighbours[way]},
+        )
+
+    def ring_sent(way, d):
+        index = d - 1 if way == 0 else d
+        ref = ring.at[way, :, index]
+        return remote(
+            ref, ref, ring_send.at[way, index], line_recv.at[0, 0], {"fs": neighbours[way]}
+        )
+
+    def extra(p):
+        return int(isinstance(p, int) and p == q)
 
     def source_of(half, i, p):
         if isinstance(p, int) and p == q:
@@ -243,7 +279,7 @@
         return remote(
             source_of(half, peer, p),
             first_in.at[at],
-            first_send.at[at],
+            first_send.at[half, k - 1, extra(p)],
             first_recv.at[at],
             {"tp": device},
         )
@@ -252,12 +288,32 @@
         _, device = second_peer(half, k)
         slot = second_in.at[half, position, p]
         at = (half, k - 1, p)
-        return remote(slot, slot, second_send.at[at], second_recv.at[at], {"tp": device})
+        return remote(
+            slot, slot, second_send.at[half, k - 1, extra(p)], second_recv.at[at], {"tp": device}
+        )
 
     def third_copy(half, k, p, shown):
         _, device = first_peer(half, k)
         ref = target_of(half, shown, p)
-        at = (half, k - 1, p)
+        at = (half, k - 1, extra(p))
+        return remote(ref, ref, third_send.at[at], third_recv.at[at], {"tp": device})
+
+    def first_sent(half, k, skip):
+        peer, device = first_peer(half, k)
+        ref = rows_s.at[block_of(half, peer), pl.ds(skip * cut, model - skip * cut)]
+        at = (half, k - 1, 0)
+        return remote(ref, ref, first_send.at[at], first_recv.at[at], {"tp": device})
+
+    def second_sent(half, k, skip):
+        _, device = second_peer(half, k)
+        ref = second_in.at[half, seconds[half], pl.ds(skip, q - skip)]
+        at = (half, k - 1, 0)
+        return remote(ref, ref, second_send.at[at], second_recv.at[at], {"tp": device})
+
+    def third_done(half, k, shown, skip):
+        _, device = first_peer(half, k)
+        ref = rows_out.at[block_of(half, shown), pl.ds(skip * cut, model - skip * cut)]
+        at = (half, k - 1, 0)
         return remote(ref, ref, third_send.at[at], third_recv.at[at], {"tp": device})
 
     def help_copy():
@@ -267,14 +323,18 @@
 
     def back_copy(half, i):
         device = jnp.where(z == 1, neighbours[1], neighbours[0])
-        at = (half, i)
         return remote(
             help_out.at[block_of(half, i)],
             rows_out.at[piece(half, i, 0)],
-            back_send.at[at],
-            back_recv.at[at],
+            back_send.at[0],
+            back_recv.at[0],
             {"fs": device},
         )
+
+    def back_done():
+        device = jnp.where(z == 1, neighbours[1], neighbours[0])
+        target = rows_out.at[:, pl.ds(0, cut)]
+        return remote(help_out, target, back_send.at[0], back_recv.at[0], {"fs": device})
 
     def small_pair():
         return remote(small_v, small_in, small_send.at[2, 0], small_recv.at[z], {"fs": partner})
@@ -340,8 +400,7 @@
             )
 
     load_rows(1).start()
-    for c in range(n):
-        load_cot(c).start()
+    load_cot().start()
     load_rows(0).start()
     for which in range(4):
         load_mix(which).start()
@@ -350,6 +409,7 @@
 
     expected = 1 + 2 * (side - 1) + jnp.where(z < last, 1, 0) + jnp.where(z > 0, 1, 0)
     pl.semaphore_wait(barrier, expected)
+    wait_weights()
 
     block = math.gcd(tokens, FORWARD_ROWS)
 
@@ -379,7 +439,7 @@
 
     def middle_earlier(c):
         value, taps, shifted, mixed, sig = mixing(c)
-        cot = cot_v[c].astype(F32)
+        cot = cot_v[:, columns(c)].astype(F32)
         grads[c, :, w:] = (cot * (mixed * sig)).astype(BF16)
         mixed_grad = cot * value * sig * (1.0 + mixed * (1.0 - sig))
         total = taps[count - 1] * mixed_grad
@@ -407,8 +467,10 @@
 
         lax.fori_loop(0, model // wide, body, 0)
 
+    skips = jnp.logical_and(helped, at_end)
+
     def kept(p):
-        return jnp.logical_not(jnp.logical_and(helped, jnp.logical_and(at_end, p == 0)))
+        return jnp.logical_not(jnp.logical_and(skips, p == 0))
 
     def start_first(p):
         @pl.when(kept(p))
@@ -422,7 +484,11 @@
             help_copy().start()
 
     def last_rows(c):
-        def body(p, carry):
+        late = q // 2
+
+        def body(turn, carry):
+            moved = jnp.where(turn < late, turn + 1, jnp.where(turn == late, 0, turn))
+            p = jnp.where(skips, moved, turn)
             cols = pl.ds(pl.multiple_of(p * cut, cut), cut)
             rows_s[:, cols] = (acc[:, cols] + rows_part(c, tail, cols)).astype(BF16)
             start_first(p)
@@ -467,18 +533,17 @@
         @pl.when(c == 0)
         def _():
             load_rows(1).wait()
+            load_cot().wait()
             for which in range(4):
                 load_mix(which).wait()
             load_sum(0).wait()
             load_sum(1).wait()
             transpose_rows()
 
-        for o in range(chips):
-            pair_copy(o, 1 - core, c).wait_recv()
+        pair_received(c).wait_recv()
         forward(earlier_v, c)
 
     def compute_second(c):
-        load_cot(c).wait()
         middle_earlier(c)
 
         @pl.when(jnp.logical_and(c < n - tail, lax.rem(c, group) == group - 1))
@@ -505,7 +570,7 @@
         def _():
             line_copy(way, o, c).start()
 
-        pair_copy(o, core, c).start()
+        pair_copy(o, c).start()
 
     def terms_of(c, d):
         rows = pl.ds(pl.multiple_of(d * depth, depth), depth)
@@ -520,10 +585,10 @@
 
         @pl.when(jnp.logical_not(first_on_line))
         def _():
-            ring_copy(way, c, d).wait_recv()
+            ring_copy(way, c, d, z).wait_recv()
             slot[...] = (terms_of(c, d) + slot[...].astype(F32)).astype(BF16)
 
-        ring_copy(way, c, d).start()
+        ring_copy(way, c, d, z + 1 if way == 0 else z - 1).start()
 
     def push_up(c, carry):
         for d in range(last, 0, -1):
@@ -552,18 +617,18 @@
 
         @pl.when(z == 0)
         def _():
-            ring_copy(1, c, z).wait_recv()
+            ring_copy(1, c, z, z).wait_recv()
             add(base + ring_slot(1, c, z)[...].astype(F32))
 
         @pl.when(z == last)
         def _():
-            ring_copy(0, c, z).wait_recv()
+            ring_copy(0, c, z, z).wait_recv()
             add(base + ring_slot(0, c, z)[...].astype(F32))
 
         @pl.when(jnp.logical_and(z > 0, z < last))
         def _():
-            ring_copy(0, c, z).wait_recv()
-            ring_copy(1, c, z).wait_recv()
+            ring_copy(0, c, z, z).wait_recv()
+            ring_copy(1, c, z, z).wait_recv()
             add(
                 base
                 + ring_slot(0, c, z)[...].astype(F32)
@@ -579,16 +644,18 @@
 
     def pushed(i, hops):
         turn = i - (n - 1)
-        near = jnp.clip(jnp.maximum(3 + (turn - 1) // 2, turn - 2), 0, n)
+        near = jnp.maximum(jnp.minimum(3 + (turn - 1) // 2, n - 2), turn - 3)
         near = jnp.where(turn >= 1, near, 0)
-        after = jnp.where(hops == 1, near, jnp.clip(turn + 1 - 2 * hops, 0, n))
+        turn -= 2 * (hops - 2)
+        distant = jnp.maximum(jnp.minimum(turn - 3, n - 2), turn - 4)
+        after = jnp.clip(jnp.where(hops == 1, near, distant), 0, n)
         return jnp.where(hops == 0, termed(i), after)
 
     batch = math.gcd(q, 2)
     rounds = q // batch
 
     hold = jnp.where(helper, rounds - 1, 0)
-    turns = max(n + 4, n + 2 * (last - 1), 6 + 2 * last, 3 * rounds, 2 * rounds + 3)
+    turns = max(n + 5, n - 1 + 2 * last, 2 * rounds + last + 1, 3 * rounds, 2 * rounds + 3)
     end = n - 1 + turns
 
     def exchange(j):
@@ -658,10 +725,6 @@
     def exchange_send(half, p):
         for k in range(1, side):
             third_copy(half, k, p, firsts[half]).start()
-
-    def exchange_third(half, p):
-        for k in range(1, side):
-            third_copy(half, k, p, lax.rem(firsts[half] + side - k, side)).wait_recv()
 
     def finish_small():
         for c in range(n):
@@ -674,60 +737,57 @@
             bias_out[:, cols] = bias_sum_ref[:, cols] + total[count : count + 1]
         small_pair().wait_send()
 
-    def drain_gather(c, carry):
-        def over_chips(d, inner):
-            pair_copy(d, core, c).wait_send()
-
-            @pl.when(jnp.logical_and(d <= z, z < last))
-            def _():
-                line_copy(0, d, c).wait_send()
-
-            @pl.when(jnp.logical_and(d >= z, z > 0))
-            def _():
-                line_copy(1, d, c).wait_send()
-
-            return inner
-
-        return lax.fori_loop(0, chips, over_chips, carry)
-
-    def drain_ring(c, carry):
+    def drain_gather(d, carry):
+        @pl.when(jnp.logical_and(d <= z, z < last))
+        def _():
+            line_sent(0, d).wait_send()
+
+        @pl.when(jnp.logical_and(d >= z, z > 0))
+        def _():
+            line_sent(1, d).wait_send()
+
+        return carry
+
+    def drain_ring():
         for d in range(chips):
             if d > 0:
 
                 @pl.when(d > z)
                 def _():
-                    ring_copy(0, c, d).wait_send()
+                    ring_sent(0, d).wait_send()
 
             if d < last:
 
                 @pl.when(d < z)
                 def _():
-                    ring_copy(1, c, d).wait_send()
-
-        return carry
+                    ring_sent(1, d).wait_send()
+
+    def each_kept(action):
+        for skip, here in ((0, jnp.logical_not(skips)), (1, skips)):
+            if skip == 0 or helped:
+
+                @pl.when(here)
+                def _():
+                    for half in range(2):
+                        for k in range(1, side):
+                            action(half, k, skip)
 
     def drain_first():
-        for p in range(q):
-
-            @pl.when(kept(p))
-            def _():
-                for half in range(2):
-                    for k in range(1, side):
-                        first_copy(half, k, p).wait_send()
+        each_kept(lambda half, k, skip: first_sent(half, k, skip).wait_send())
 
     def drain_second():
-        for p in range(q):
-
-            @pl.when(kept(p))
-            def _():
-                for half in range(2):
-                    for k in range(1, side):
-                        second_copy(half, k, p, seconds[half]).wait_send()
+        each_kept(lambda half, k, skip: second_sent(half, k, skip).wait_send())
+
+    def drain_third(half, k, skip):
+        shown = lax.rem(firsts[half] + side - k, side)
+        third_done(half, k, shown, skip).wait_recv()
+        third_done(half, k, firsts[half], skip).wait_send()
 
     def drain_early(j):
         @pl.when(j == rounds)
         def _():
-            lax.fori_loop(0, n, drain_gather, 0)
+            pair_sent().wait_send()
+            lax.fori_loop(0, chips, drain_gather, 0)
             for c in range(max(n - 2, 0), n):
                 term_copy(c).wait_send()
 
@@ -736,14 +796,10 @@
             drain_first()
 
     def drain_late():
-        lax.fori_loop(0, n - 1, drain_ring, 0)
         drain_second()
         finish_small()
 
     def send_own(c, carry):
-        load_weight(c, 0).wait()
-        load_weight(c, 1).wait()
-
         @pl.when(z < last)
         def _():
             line_copy(0, z, c).start()
@@ -752,7 +808,7 @@
         def _():
             line_copy(1, z, c).start()
 
-        pair_copy(z, core, c).start()
+        pair_copy(z, c).start()
         return carry
 
     @pl.when(at_end)
@@ -784,25 +840,24 @@
         def _():
             compute_first(i)
 
+        lax.fori_loop(termed(i - 1), termed(i), wait_terms, 0)
+        @pl.when(i == n)
+        def _():
+            send_small()
+
+        turn = i - (n - 1) - 2 * rounds
+
+        @pl.when(jnp.logical_and(turn >= 1, turn <= last))
+        def _():
+            pass_small(turn)
+
+        lax.fori_loop(pushed(i - 1, z), pushed(i, z), push_up, 0)
+        lax.fori_loop(pushed(i - 1, last - z), pushed(i, last - z), push_down, 0)
+        hops = jnp.where(at_end, 2, far)
+        lax.fori_loop(pushed(i - 2, hops), pushed(i - 1, hops), finish_sum, 0)
+
         drain_early(i - (n - 1))
         exchange(i - (n - 1))
-        lax.fori_loop(termed(i - 1), termed(i), wait_terms, 0)
-        @pl.when(i == n)
-        def _():
-            send_small()
-
-        turn = i - (n + 4)
-        inside = jnp.logical_and(turn >= 2, turn <= 2 * last)
-
-        @pl.when(jnp.logical_and(inside, lax.rem(turn, 2) == 0))
-        def _():
-            pass_small(turn // 2)
-
-        lax.fori_loop(pushed(i - 1, z), pushed(i, z), push_up, 0)
-        lax.fori_loop(pushed(i - 1, last - z), pushed(i, last - z), push_down, 0)
-        finish = jnp.where(at_end, i - 1, i)
-        hops = jnp.where(at_end, 2, far)
-        lax.fori_loop(pushed(finish - 1, hops), pushed(finish, hops), finish_sum, 0)
 
         @pl.when(i == end)
         def _():
@@ -820,7 +875,7 @@
 
     lax.fori_loop(0, end + last + 1, step, 0)
 
-    lax.fori_loop(n - 1, n, drain_ring, 0)
+    drain_ring()
 
     def drain_small(o, carry):
         @pl.when(jnp.logical_and(o <= z, z < last))
@@ -834,41 +889,46 @@
         return carry
 
     lax.fori_loop(0, chips, drain_small, 0)
-    for p in range(q):
-
-        @pl.when(kept(p))
-        def _():
-            for half in range(2):
-                exchange_third(half, p)
-                for k in range(1, side):
-                    third_copy(half, k, p, firsts[half]).wait_send()
+    each_kept(drain_third)
 
     if helped:
 
         @pl.when(at_end)
         def _():
             help_copy().wait_send()
-            for half in range(2):
-                for i in range(side):
-                    back_copy(half, i).wait_recv()
+            back_done().wait_recv()
 
         @pl.when(helper)
         def _():
+            back_done().wait_send()
             for half in range(2):
                 for k in range(1, side):
                     first_copy(half, k, q).wait_send()
                     second_copy(half, k, q, seconds[half]).wait_send()
                     third_copy(half, k, q, firsts[half]).wait_send()
-                for i in range(side):
-                    back_copy(half, i).wait_send()
+
+
+STORES = 4
+
+
+def stores_of(rows):
+    return STORES if rows % (16 * STORES) == 0 else 1
 
 
 def store_kernel(*refs):
     count = len(refs) // 2
     sources, targets, sems = refs[:count], refs[count : 2 * count], refs[-1]
-    copies = [
-        pltpu.make_async_copy(sources[at], targets[at], sems.at[at]) for at in range(count)
-    ]
+    copies = []
+    for at in range(count):
+        rows = sources[at].shape[0]
+        parts = stores_of(rows)
+        for part in range(parts):
+            block = pl.ds(part * (rows // parts), rows // parts)
+            copies.append(
+                pltpu.make_async_copy(
+                    sources[at].at[block], targets[at].at[block], sems.at[at, part]
+                )
+            )
     for copy in copies:
         copy.start()
     for copy in copies:
@@ -916,7 +976,7 @@
             pltpu.VMEM((tokens, model), BF16),
             pltpu.VMEM((tokens, model), BF16),
             pltpu.VMEM((model, tokens), BF16),
-            pltpu.VMEM((n, tokens, w), BF16),
+            pltpu.VMEM((tokens, width), BF16),
             pltpu.VMEM((n, model, 2 * w), BF16),
             pltpu.VMEM((tokens, 2 * w), BF16),
             pltpu.VMEM((n, tokens, 2 * w), BF16),
@@ -930,8 +990,8 @@
             pltpu.VMEM((tokens, cut), BF16),
             dma((1,)),
             dma((1,)),
-            dma((2, side)),
-            dma((2, side)),
+            dma((1,)),
+            dma((1,)),
             pltpu.VMEM((2, links, q + 1, r, cut), BF16),
             pltpu.VMEM((2, side, q + 1, r, cut), BF16),
             pltpu.VMEM((n, 8 * -(-(taps + 1) // 8), w), F32),
@@ -942,21 +1002,26 @@
             pltpu.VMEM((taps, width), F32),
             pltpu.VMEM((1, width), F32),
             dma((4,)),
-            dma((n, 2)),
+            dma((2,)),
+            dma((2,)),
+            dma((1,)),
+            dma((2,)),
+            dma((2, chips)),
+            dma((n, chips + 2)),
+            dma((1,)),
+            dma((n,)),
             dma((2,)),
             dma((n,)),
-            dma((2,)),
-            dma((2, n, chips)),
-            dma((n, chips)),
-            dma((n, chips)),
-            dma((n, chips)),
-            dma((n,)),
-            dma((n,)),
-            dma((2, n, max(chips - 1, 1))),
-            dma((2, n, max(chips - 1, 1))),
-        ]
-        + [dma((2, links, q + 1))] * 6
-        + [dma((3, chips)), dma((chips,))],
+            dma((2, max(chips - 1, 1))),
+            dma((2, links, 2)),
+            dma((2, links, q + 1)),
+            dma((2, links, 2)),
+            dma((2, links, q + 1)),
+            dma((2, links, 2)),
+            dma((2, links, 2)),
+            dma((3, chips)),
+            dma((chips,)),
+        ],
         compiler_params=pltpu.CompilerParams(
             collective_id=0, has_side_effects=True, vmem_limit_bytes=VMEM_BYTES
         ),
@@ -978,7 +1043,7 @@
         out_shape=tuple(jax.ShapeDtypeStruct(out.shape, out.dtype) for out in outs),
         in_specs=[whole] * len(outs),
         out_specs=(far,) * len(outs),
-        scratch_shapes=[dma((len(outs),))],
+        scratch_shapes=[dma((len(outs), STORES))],
         compiler_params=pltpu.CompilerParams(vmem_limit_bytes=1024 * 1024),
     )(*[pltpu.with_memory_space_constraint(out, pltpu.VMEM) for out in outs])
     return stored[:5] + (stored[5][0],)

time: 133 us -> 130 us (0.977)
  Pallas kernels: 132 us -> 129 us
    pallas_call x1, Pallas kernels: 129 us -> 126 us  [on_device(): pl.pallas_call(functools.partial(kernel, sizes), out_shape=(pltpu.VMEM((t...]
where the time goes in v4:
time: 130 us
  Pallas kernels  129 us (99%)
    pallas_call x1, Pallas kernels, on_device(): pl.pallas_call(functools.partial(kernel, sizes), out_shape=(pltpu.VMEM((t...  126 us
    pallas_call x1, Pallas kernels, on_device(): pl.pallas_call(store_kernel, out_shape=tuple((jax.ShapeDtypeStruct(out.sh...  3.02 us

profile of v4, /device:TPU:0, one launch (start us, length us, event | category | flops | bytes accessed | tf_op | source)
XLA Modules:
  0.0 129.7 jit_solution(17803604482684610938)
XLA Ops:
  0.6 126.0 %shard_map.154 = (bf16[768,1024]{1,0:T(8,128)(2,1)S(1)}, bf16[768,2048]{1,0:T(8,128)(2,1)S(1)}, f32[256,1024]{1,0:T(8,128)S(1)}, f32[256,1024]{1,0:T(8,128)S(1)}...) custom-call(bf16[768,2048]{1,0:T(8,128)(2,1)} %later_hbm.1, bf16[768,2048]{1,0:T(8,128)(2,1)} %earlier_hbm.1, ...), custom_call_target="tpu_custom_call" | custom-call | tf_op jit(solution)/shard_map/pallas_call | solution.py:963
  126.6 3.0 %shard_map.155 = (bf16[768,1024]{1,0:T(8,128)(2,1)}, bf16[768,2048]{1,0:T(8,128)(2,1)}, f32[256,1024]{1,0:T(8,128)}, f32[256,1024]{1,0:T(8,128)}, f32[3,1024]{1,0:T(4,128)}, /*index=5*/f32[1,1024]{1,0:T(1,128)}) custom-call(bf16[768,1024]{1,0:T(8,128)(2,1)S(1)} %get-tuple-element.18.refs_0_, bf16[768,2048]{1,0:T(8,128)(2,1)S(1)} %get-tuple-element.19.refs_1_, ...), custom_call_target="tpu_custom_call" | custom-call | tf_op jit(solution)/shard_map/pallas_call | solution.py:1041

commit v5 on v4

--- a/solution.py
+++ b/solution.py
@@ -46,6 +46,7 @@
         self.taps = taps
         self.group = math.gcd(self.n, 2)
         self.tail = min(self.n, 2 * self.group)
+        self.lead = min(self.n, 1)
         self.r = tokens // (2 * self.side)
         self.q = max(q for q in (1, 2, 4, 8) if model % (128 * q) == 0)
         self.cut = model // self.q
@@ -121,7 +122,7 @@
     small_recv,
 ):
     n, w, q, r, cut = sizes.n, sizes.w, sizes.q, sizes.r, sizes.cut
-    group, tail = sizes.group, sizes.tail
+    group, tail, lead = sizes.group, sizes.tail, sizes.lead
     chips, side, depth = sizes.chips, sizes.side, sizes.depth
     fs_size, tokens, model = sizes.fs_size, sizes.tokens, sizes.model
     count = sizes.taps
@@ -545,6 +546,7 @@
 
     def compute_second(c):
         middle_earlier(c)
+        lax.fori_loop(made(c - 1), jnp.where(c < n - 1, made(c), made(c - 1)), make_terms, 0)
 
         @pl.when(jnp.logical_and(c < n - tail, lax.rem(c, group) == group - 1))
         def _():
@@ -641,6 +643,9 @@
 
     def termed(i):
         return jnp.where(i >= n, n, jnp.clip(i, 0, max(n - 2, 0)))
+
+    def made(i):
+        return jnp.where(i >= n, n, jnp.clip(i + 1, 0, max(n - 2, 0)))
 
     def pushed(i, hops):
         turn = i - (n - 1)
@@ -799,48 +804,55 @@
         drain_second()
         finish_small()
 
-    def send_own(c, carry):
-        @pl.when(z < last)
-        def _():
-            line_copy(0, z, c).start()
-
-        @pl.when(z > 0)
-        def _():
-            line_copy(1, z, c).start()
+    heavy = jnp.where(2 * z < last, 1, 0)
+
+    def send_heavy(c):
+        for way, goes_on in ((0, z < last), (1, z > 0)):
+
+            @pl.when(jnp.logical_and(heavy == way, goes_on))
+            def _():
+                line_copy(way, z, c).start()
+
+    def send_light(c):
+        for way, goes_on in ((0, z < last), (1, z > 0)):
+
+            @pl.when(jnp.logical_and(heavy != way, goes_on))
+            def _():
+                line_copy(way, z, c).start()
 
         pair_copy(z, c).start()
+
+    def send_all(c, carry):
+        send_heavy(c)
+        send_light(c)
         return carry
 
     @pl.when(at_end)
     def _():
-        lax.fori_loop(0, n, send_own, 0)
+        lax.fori_loop(0, n, send_all, 0)
+
+    @pl.when(jnp.logical_not(at_end))
+    def _():
+        for c in range(lead):
+            send_heavy(c)
 
     def step(s, carry):
         i = s - far
 
+        @pl.when(jnp.logical_and(s + lead < n, jnp.logical_not(at_end)))
+        def _():
+            send_heavy(s + lead)
+
         @pl.when(jnp.logical_and(s < n, jnp.logical_not(at_end)))
         def _():
-            send_own(s, 0)
-
-        for k in range(1, chips):
-            c = s - k
-            inside = jnp.logical_and(c >= 0, c < n)
-
-            @pl.when(jnp.logical_and(inside, z - k >= 0))
-            def _():
-                arrive(0, z - k, c, z < last)
-
-            @pl.when(jnp.logical_and(inside, z + k <= last))
-            def _():
-                arrive(1, z + k, c, z > 0)
-
-        lax.fori_loop(termed(i - 1), termed(i), make_terms, 0)
-
-        @pl.when(jnp.logical_and(i >= 0, i < n))
-        def _():
-            compute_first(i)
-
-        lax.fori_loop(termed(i - 1), termed(i), wait_terms, 0)
+            send_light(s)
+
+        @pl.when(i == n)
+        def _():
+            lax.fori_loop(made(n - 1), n, make_terms, 0)
+
+        early = jnp.logical_or(at_end, i >= n)
+        lax.fori_loop(termed(i - 1), jnp.where(early, termed(i), termed(i - 1)), wait_terms, 0)
         @pl.when(i == n)
         def _():
             send_small()
@@ -856,6 +868,23 @@
         hops = jnp.where(at_end, 2, far)
         lax.fori_loop(pushed(i - 2, hops), pushed(i - 1, hops), finish_sum, 0)
 
+        for k in range(1, chips):
+            c = s - k
+            inside = jnp.logical_and(c >= 0, c < n)
+
+            @pl.when(jnp.logical_and(inside, z - k >= 0))
+            def _():
+                arrive(0, z - k, c, z < last)
+
+            @pl.when(jnp.logical_and(inside, z + k <= last))
+            def _():
+                arrive(1, z + k, c, z > 0)
+
+        @pl.when(jnp.logical_and(i >= 0, i < n))
+        def _():
+            compute_first(i)
+
+        lax.fori_loop(jnp.where(early, termed(i), termed(i - 1)), termed(i), wait_terms, 0)
         drain_early(i - (n - 1))
         exchange(i - (n - 1))
 

time: 130 us -> 129 us (level)
  no operation moved by 1% of the time
where the time goes in v5:
time: 129 us
  Pallas kernels  129 us (100%)
    pallas_call x1, Pallas kernels, on_device(): pl.pallas_call(functools.partial(kernel, sizes), out_shape=(pltpu.VMEM((t...  126 us
    pallas_call x1, Pallas kernels, on_device(): pl.pallas_call(store_kernel, out_shape=tuple((jax.ShapeDtypeStruct(out.sh...  3.02 us

profile of v5, /device:TPU:0, one launch (start us, length us, event | category | flops | bytes accessed | tf_op | source)
XLA Modules:
  0.0 129.3 jit_solution(14634963992637424423)
XLA Ops:
  0.6 125.6 %shard_map.154 = (bf16[768,1024]{1,0:T(8,128)(2,1)S(1)}, bf16[768,2048]{1,0:T(8,128)(2,1)S(1)}, f32[256,1024]{1,0:T(8,128)S(1)}, f32[256,1024]{1,0:T(8,128)S(1)}...) custom-call(bf16[768,2048]{1,0:T(8,128)(2,1)} %later_hbm.1, bf16[768,2048]{1,0:T(8,128)(2,1)} %earlier_hbm.1, ...), custom_call_target="tpu_custom_call" | custom-call | tf_op jit(solution)/shard_map/pallas_call | solution.py:992
  126.2 3.0 %shard_map.155 = (bf16[768,1024]{1,0:T(8,128)(2,1)}, bf16[768,2048]{1,0:T(8,128)(2,1)}, f32[256,1024]{1,0:T(8,128)}, f32[256,1024]{1,0:T(8,128)}, f32[3,1024]{1,0:T(4,128)}, /*index=5*/f32[1,1024]{1,0:T(1,128)}) custom-call(bf16[768,1024]{1,0:T(8,128)(2,1)S(1)} %get-tuple-element.18.refs_0_, bf16[768,2048]{1,0:T(8,128)(2,1)S(1)} %get-tuple-element.19.refs_1_, ...), custom_call_target="tpu_custom_call" | custom-call | tf_op jit(solution)/shard_map/pallas_call | solution.py:1070
